TPU v7x, 128 devices: a whole 4x4x4 slice. The times are simulated.
128 devices in a mesh: sp: 64 (over z, y, x), tp: 2 (over core).
Axes of the slice: x: 4, y: 4, z: 4, core: 2. Of those that a mesh axis runs over, the one named last changes fastest.
Arguments:
- projected_queries: bfloat16 [32768, 1024], P('sp', 'tp'), may hold values from -6 to 6
- projected_keys: bfloat16 [32768, 1024], P('sp', 'tp'), may hold values from -6 to 6
- projected_values: bfloat16 [32768, 1024], P('sp', 'tp'), may hold values from -6 to 6
- output_gate_values: bfloat16 [32768, 1024], P('sp', 'tp'), may hold values from -6 to 6
- write_strength_logits: bfloat16 [32768, 8], P('sp', 'tp'), may hold values from -6.5 to 3
- decay_input_logits: bfloat16 [32768, 8], P('sp', 'tp'), may hold values from -5 to 5
- head_rate_logarithm: float32 [8], P('tp'), may hold values from -8 to 2.3
- extra_log_decay: float32 [32768, 8], P('sp', 'tp'), may hold values from -0.7 to 0
- per_head_norm_gain: float32 [128], replicated, may hold values from 0.1 to 1.9
- output_matrix: bfloat16 [1024, 2048], replicated, may hold values from -0.1875 to 0.1875
- residual: bfloat16 [32768, 2048], P(('sp', 'tp')), may hold values from -6 to 6
- mixture_norm_gain: float32 [2048], replicated, may hold values from 0.1 to 1.9
- selected_expert_index: int32 [32768, 4], P(('sp', 'tp')), may hold values from 0 to 127, all different within a row; in each aligned block of 256 rows (0 to 255, 256 to 511, ...) at most 12 rows name the same one
- routing_weight: float32 [32768, 4], P(('sp', 'tp')), may hold values from 0.1 to 0.9
- routed_gate_weight: bfloat16 [128, 2048, 512], P(('sp', 'tp')), may hold values from -0.125 to 0.125
- routed_up_weight: bfloat16 [128, 2048, 512], P(('sp', 'tp')), may hold values from -0.125 to 0.125
- routed_down_weight: bfloat16 [128, 512, 2048], P(('sp', 'tp')), may hold values from -0.25 to 0.25
- common_gate_weight: bfloat16 [2048, 512], replicated, may hold values from -0.125 to 0.125
- common_up_weight: bfloat16 [2048, 512], replicated, may hold values from -0.125 to 0.125
- common_down_weight: bfloat16 [512, 2048], replicated, may hold values from -0.25 to 0.25
Outputs:
- block_out: bfloat16 [32768, 2048], P(('sp', 'tp'))
Inputs may be any that keep to these rules, and one draw needn't show every extreme that they name: `selected_expert_index`: each row names 4 different experts. Among the rows that one device holds, no expert is named more than 12 times.
All inputs are finite; a program needn't handle non-finite values.
Results may differ from a plain program's by a relative error of at most 0.008.
Values may be sent and summed in bfloat16 or wider, within the bound.
A program may use at most 192 MiB of HBM per device.

v0:
```python
import jax
import jax.numpy as jnp
from jax import lax
from jax.sharding import Mesh
from jax.sharding import PartitionSpec as P

TOP_K = 4
SPAN = 64
SP = ("sp_0", "sp_1", "sp_2")
SP_TP = ("sp_0", "sp_1", "sp_2", "tp")


EPS = 1e-06
HIGH = lax.Precision.HIGHEST


def nothing_yet(shard, identity):
    return jax.tree.map(
        lambda a, e: jnp.broadcast_to(jnp.asarray(e, a.dtype), a.shape), shard, identity
    )


def entering(shard, axes, combine, identity):
    before = start = nothing_yet(shard, identity)
    running = shard
    for axis in reversed(axes):
        count, mine = (lax.axis_size(axis), lax.axis_index(axis))
        pieces = jax.tree.map(lambda part: lax.all_gather(part, axis), running)
        inside, running = (start, start)
        for k in range(count):
            passed = k < mine
            running = combine(running, jax.tree.map(lambda part: part[k], pieces))
            inside = jax.tree.map(lambda new, old: jnp.where(passed, new, old), running, inside)
        before = combine(inside, before)
    return before


def items_in_groups(shard, axis, split_dim, concat_dim, work, item_dim, out_dim):
    items = jax.tree.leaves(shard)[0].shape[item_dim]
    count = 2 if items % 2 == 0 else 1
    gathered = []
    for k in range(count):
        group = jax.tree.map(
            lambda a: lax.slice_in_dim(
                a, k * (items // count), (k + 1) * (items // count), axis=item_dim
            ),
            shard,
        )
        gathered.append(
            work(
                lax.all_to_all(
                    group, axis, split_axis=split_dim, concat_axis=concat_dim, tiled=True
                )
            )
        )
    return jax.tree.map(lambda *parts: jnp.concatenate(parts, axis=out_dim), *gathered)


def unit_heads(raw, heads):
    active = jax.nn.silu(raw.astype(jnp.float32)).reshape(raw.shape[0], heads, -1)
    return active * lax.rsqrt(jnp.sum(active * active, axis=-1, keepdims=True) + EPS)


def prepare_inputs(
    projected_queries,
    projected_keys,
    projected_values,
    write_strength_logits,
    decay_input_logits,
    head_rate_logarithm,
    extra_log_decay,
):
    heads = head_rate_logarithm.shape[0]
    queries = unit_heads(projected_queries, heads)
    keys = unit_heads(projected_keys, heads)
    values = jax.nn.silu(projected_values.astype(jnp.float32)).reshape(
        projected_values.shape[0], heads, -1
    )
    beta = jax.nn.sigmoid(write_strength_logits.astype(jnp.float32))
    decay_logarithm = extra_log_decay - jnp.exp(head_rate_logarithm)[None, :] * jax.nn.softplus(
        decay_input_logits.astype(jnp.float32) - 6.0
    )
    return (queries, keys, values, beta, decay_logarithm)


def block_terms(queries, keys, values, beta, decay_logarithm):
    length, heads, width = queries.shape
    number = length // SPAN

    def split(array):
        return jnp.moveaxis(array.reshape(number, SPAN, heads, -1), 2, 0)

    q_blocks = split(queries)
    k_blocks = split(keys)
    v_blocks = split(values)
    b_blocks = split(beta[..., None])[..., 0]
    g_cumul = jnp.cumsum(split(decay_logarithm[..., None])[..., 0], axis=-1)
    place = jnp.arange(SPAN)
    causal = place[:, None] >= place[None, :]
    strict = place[:, None] > place[None, :]
    spread = jnp.where(causal, g_cumul[..., :, None] - g_cumul[..., None, :], 0.0)
    decay = jnp.where(causal, jnp.exp(spread), 0.0)
    k_beta = k_blocks * b_blocks[..., None]
    inner = jnp.einsum("hncd,hnsd->hncs", k_beta, k_blocks, precision=HIGH)
    lower = jnp.where(strict, inner * decay, 0.0) + jnp.eye(SPAN, dtype=jnp.float32)
    right = jnp.concatenate(
        [v_blocks * b_blocks[..., None], k_beta * jnp.exp(g_cumul)[..., None]], axis=-1
    )
    solved = jax.scipy.linalg.solve_triangular(lower, right, lower=True, unit_diagonal=True)
    u_part = solved[..., :width]
    w_part = solved[..., width:]
    scores = jnp.einsum("hncd,hnsd->hncs", q_blocks, k_blocks, precision=HIGH) * decay
    q_decayed = q_blocks * jnp.exp(g_cumul)[..., None]
    log_last = g_cumul[..., -1]
    k_decayed = k_blocks * jnp.exp(log_last[..., None] - g_cumul)[..., None]
    return (q_decayed, scores, u_part, w_part, k_decayed, log_last)


def run_blocks(terms, start):

    def advance(state, items):
        q_one, s_one, u_one, w_one, k_one, log_one = items
        fresh = u_one - jnp.einsum("hcd,hde->hce", w_one, state, precision=HIGH)
        result = jnp.einsum("hcd,hde->hce", q_one, state, precision=HIGH)
        result = result + jnp.einsum("hcs,hse->hce", s_one, fresh, precision=HIGH)
        state = state * jnp.exp(log_one)[:, None, None] + jnp.einsum(
            "hcd,hce->hde", k_one, fresh, precision=HIGH
        )
        return (state, result)

    items = tuple((jnp.moveaxis(array, 1, 0) for array in terms))
    _, results = lax.scan(advance, start, items)
    number, heads, span, width = results.shape
    return results.transpose(0, 2, 1, 3).reshape(number * span, heads, width)


def state_maps(terms):
    q_decayed, scores, u_part, w_part, k_decayed, log_last = terms
    heads, number, span, width = u_part.shape
    identity = jnp.broadcast_to(jnp.eye(width, dtype=jnp.float32), (heads, width, width))
    empty = jnp.zeros((heads, width, width), jnp.float32)

    def compose(pair, items):
        mapping, carried = pair
        w_one, u_one, k_one, log_one = items
        factor = jnp.exp(log_one)[:, None, None]
        erased = jnp.einsum("hcd,hde->hce", w_one, mapping, precision=HIGH)
        mapping = mapping * factor - jnp.einsum("hcd,hce->hde", k_one, erased, precision=HIGH)
        fresh = u_one - jnp.einsum("hcd,hde->hce", w_one, carried, precision=HIGH)
        carried = carried * factor + jnp.einsum("hcd,hce->hde", k_one, fresh, precision=HIGH)
        return ((mapping, carried), None)

    items = tuple((jnp.moveaxis(array, 1, 0) for array in (w_part, u_part, k_decayed, log_last)))
    (mapping, carried), _ = lax.scan(compose, (identity, empty), items)
    return (mapping, carried, identity, empty)


def chain(earlier, later):
    mapping = jnp.einsum("hij,hjk->hik", later[0], earlier[0], precision=HIGH)
    carried = jnp.einsum("hij,hjk->hik", later[0], earlier[1], precision=HIGH) + later[1]
    return (mapping, carried)


def finish(head_mix, output_gate_values, per_head_norm_gain):
    length, heads, width = head_mix.shape
    scaled = head_mix * lax.rsqrt(jnp.mean(head_mix * head_mix, axis=-1, keepdims=True) + EPS)
    gated = (
        scaled
        * per_head_norm_gain
        * jax.nn.silu(output_gate_values.astype(jnp.float32).reshape(length, heads, width))
    )
    return gated.reshape(length, heads * width).astype(jnp.bfloat16)


def normalize(stream, gain):
    wide = stream.astype(jnp.float32)
    return (wide * lax.rsqrt(jnp.mean(wide * wide, axis=-1, keepdims=True) + EPS) * gain).astype(
        jnp.bfloat16
    )


def feed_forward(rows, w_gate, w_up, w_down):
    hidden = jax.nn.silu(jnp.dot(rows, w_gate, preferred_element_type=jnp.float32))
    hidden = (hidden * jnp.dot(rows, w_up, preferred_element_type=jnp.float32)).astype(jnp.bfloat16)
    return jnp.dot(hidden, w_down, preferred_element_type=jnp.float32)


def shards(
    projected_queries,
    projected_keys,
    projected_values,
    output_gate_values,
    write_strength_logits,
    decay_input_logits,
    head_rate_logarithm,
    extra_log_decay,
    per_head_norm_gain,
    output_matrix,
    residual,
    mixture_norm_gain,
    selected_expert_index,
    routing_weight,
    routed_gate_weight,
    routed_up_weight,
    routed_down_weight,
    common_gate_weight,
    common_up_weight,
    common_down_weight,
):
    prepared_inputs = prepare_inputs(
        projected_queries,
        projected_keys,
        projected_values,
        write_strength_logits,
        decay_input_logits,
        head_rate_logarithm,
        extra_log_decay,
    )
    terms = block_terms(*prepared_inputs)
    mapping, carried, identity, empty = state_maps(terms)
    before = entering((mapping, carried), SP, chain, (identity, empty))
    heads_out = finish(run_blocks(terms, before[1]), output_gate_values, per_head_norm_gain)
    token_heads = lax.all_to_all(heads_out, "tp", split_axis=0, concat_axis=1, tiled=True)
    projected = jnp.dot(token_heads, output_matrix, preferred_element_type=jnp.float32)
    attended = (residual.astype(jnp.float32) + projected).astype(jnp.bfloat16)
    normed = normalize(attended, mixture_norm_gain)
    length = normed.shape[0]
    experts = lax.axis_size(SP) * lax.axis_size("tp")
    room = max(2, length * TOP_K * 3 // (2 * experts))
    flat_ids = selected_expert_index.reshape(-1)
    total = flat_ids.shape[0]
    onehot = (flat_ids[:, None] == jnp.arange(experts, dtype=jnp.int32)[None, :]).astype(
        jnp.bfloat16
    )
    place = jnp.arange(total, dtype=jnp.int32)
    earlier = (place[:, None] > place[None, :]).astype(jnp.bfloat16)
    before_count = jnp.dot(earlier, onehot, preferred_element_type=jnp.float32)
    slot = jnp.sum(before_count * onehot.astype(jnp.float32), axis=1).astype(jnp.int32)
    target = flat_ids * room + slot
    source = jnp.zeros((experts * room,), jnp.int32).at[target].set(place // TOP_K)
    filled = jnp.zeros((experts * room,), jnp.bool_).at[target].set(True)
    outgoing = jnp.where(filled[:, None], normed[source], jnp.zeros((), jnp.bfloat16)).reshape(
        experts, room, -1
    )

    def expert_ffn(arrived):
        flat = arrived.reshape(-1, arrived.shape[-1])
        result = feed_forward(
            flat, routed_gate_weight[0], routed_up_weight[0], routed_down_weight[0]
        ).astype(jnp.bfloat16)
        return result.reshape(arrived.shape)

    def serve(arrived):
        return lax.all_to_all(expert_ffn(arrived), SP_TP, split_axis=0, concat_axis=0, tiled=True)

    back = items_in_groups(outgoing, SP_TP, 0, 0, serve, 1, 1)
    returned_rows = back.reshape(experts * room, -1)[target].reshape(length, TOP_K, -1)
    routed = jnp.einsum("rk,rkd->rd", routing_weight, returned_rows.astype(jnp.float32))
    shared = feed_forward(normed, common_gate_weight, common_up_weight, common_down_weight)
    return (attended.astype(jnp.float32) + shared + routed).astype(jnp.bfloat16)


def solution(mesh):
    finer = Mesh(mesh.devices.reshape(4, 4, 4, mesh.shape["tp"]), ("sp_0", "sp_1", "sp_2", "tp"))
    in_specs = (
        P(SP, "tp"),
        P(SP, "tp"),
        P(SP, "tp"),
        P(SP, "tp"),
        P(SP, "tp"),
        P(SP, "tp"),
        P("tp"),
        P(SP, "tp"),
        P(),
        P(),
        P(SP_TP, None),
        P(),
        P(SP_TP, None),
        P(SP_TP, None),
        P(SP_TP, None, None),
        P(SP_TP, None, None),
        P(SP_TP, None, None),
        P(),
        P(),
        P(),
    )
    out_specs = P(SP_TP, None)
    return jax.shard_map(
        shards, mesh=finer, in_specs=in_specs, out_specs=out_specs, check_vma=False
    )
```

profile of v0, /device:TPU:1, one launch (start us, length us, event | category | flops | bytes accessed | tf_op | source)
XLA Modules:
  0.0 804.6 jit_solution(5793430192315798224)
XLA Ops:
  9.5 2.7 fusion.188
  12.2 2.6 mul.218
  16.8 2.5 reshape.170
  19.5 5.1 fusion.76
  24.7 158.7 %custom-call.4 = f32[4,8,1,64,64]{3,4,2,1,0:T(8,128)} custom-call(f32[4,8,1,64,64]{4,3,2,1,0:T(8,128)} %fusion.76), custom_call_target="InvertDiagBlocksLowerTriangular" | custom-call | tf_op jit(solution)/shard_map/jit(_solve_triangular)/vmap(vmap())/triangular_solve | solution.py:109
  184.6 2.5 reshape_reshape.3
  195.7 45.6 %while.26 = (s32[]{:T(128)}, f32[4,128,128]{2,1,0:T(8,128)S(1)}, f32[4,128,128]{2,1,0:T(8,128)S(1)}, f32[8,4]{1,0:T(8,128)S(1)}, f32[8,4,64,128]{3,2,1,0:T(8,128...) while((s32[]{:T(128)}, f32[4,128,128]{2,1,0:T(8,128)S(1)}, ...), condition=%wide.region_3.4_spmd.clone, body=%wide.region_2.3_spmd.clone.sunk | while | flops 201752576 | bytes 2755244 | solution.py:154
  243.1 24.3 %all-gather.13.cloned.1.call-done = f32[16,128,128]{2,1,0:T(8,128)} async-done(((f32[4,128,128]{2,1,0:T(8,128)}), f32[16,128,128]{2,1,0:T(8,128)}) %all-gather.13.cloned.1.call-update) | async-done | bytes 1048592 | tf_op jit(solution)/shard_map/all_gather | solution.py:28
  267.4 26.1 %all-gather.19.cloned.1.call-done = f32[16,128,128]{2,1,0:T(8,128)} async-done(((f32[4,128,128]{2,1,0:T(8,128)}), f32[16,128,128]{2,1,0:T(8,128)}) %all-gather.19.cloned.1.call-update) | async-done | bytes 1048592 | tf_op jit(solution)/shard_map/all_gather | solution.py:28
  304.6 4.3 scatter_custom_fusion.1
  310.6 13.5 %all-gather.21.cloned.1.call-done = f32[16,128,128]{2,1,0:T(8,128)} async-done(((f32[4,128,128]{2,1,0:T(8,128)}), f32[16,128,128]{2,1,0:T(8,128)}) %all-gather.21.cloned.1.call-update) | async-done | bytes 1048592 | tf_op jit(solution)/shard_map/all_gather | solution.py:28
  324.1 26.0 %all-gather.15.cloned.1.call-done = f32[16,128,128]{2,1,0:T(8,128)} async-done(((f32[4,128,128]{2,1,0:T(8,128)}), f32[16,128,128]{2,1,0:T(8,128)}) %all-gather.15.cloned.1.call-update) | async-done | bytes 1048592 | tf_op jit(solution)/shard_map/all_gather | solution.py:28
  356.5 2.6 mul.233
  359.1 2.6 reduce_sum.46
  361.6 2.6 reshape.171
  365.3 2.9 multiply_bitcast_fusion
  372.8 4.8 scatter_custom_fusion
  377.7 4.5 fusion.63
  387.1 19.9 %all-gather.17.cloned.1.call-done = f32[16,128,128]{2,1,0:T(8,128)} async-done(((f32[4,128,128]{2,1,0:T(8,128)}), f32[16,128,128]{2,1,0:T(8,128)}) %all-gather.17.cloned.1.call-update) | async-done | bytes 1048592 | tf_op jit(solution)/shard_map/all_gather | solution.py:28
  413.8 48.5 %while.25 = (s32[]{:T(128)}, f32[4,128,128]{2,1,0:T(8,128)S(1)}, f32[8,4,64,128]{3,2,1,0:T(8,128)S(1)}, f32[8,4]{1,0:T(8,128)}, f32[8,4,64,128]{3,2,1,0:T(8,128)...) while((s32[]{:T(128)}, f32[4,128,128]{2,1,0:T(8,128)S(1)}, ...), condition=%wide.region_6.7_spmd, body=%wide.region_5.6_spmd.sunk | while | flops 176357376 | bytes 2754721 | solution.py:132
  464.7 6.7 all_to_all.39
  471.4 3.9 fusion.37
  476.6 7.1 gather_fusion
  483.7 10.6 %gather.9 = bf16[128,12,2048]{2,1,0:T(8,128)(2,1)} reshape(bf16[1536,2048]{1,0:T(8,128)(2,1)} %gather_fusion) | data formatting | bytes 12582912 | tf_op jit(solution)/shard_map/gather | solution.py:242
  494.3 7.4 broadcast_select_fusion
  501.7 7.1 fusion.190
  508.8 61.0 %all_to_all.40 = bf16[128,6,2048]{2,1,0:T(8,128)(2,1)} all-to-all(bf16[128,6,2048]{2,1,0:T(8,128)(2,1)S(1)} %get-tuple-element.229), channel_id=1, replica_groups=mesh['sp_0'=4,'sp_1'=4,'sp_2'=4,'tp'=2] {'sp_0','sp_1','sp_2','tp'}, dimensions={0} | all-to-all | bytes 6291456 | tf_op jit(solution)/shard_map/all_to_all | solution.py:51
  569.9 5.5 all-to-all-start.3
  575.4 6.4 reshape.173
  581.8 5.5 fusion.52
  587.3 8.1 %convolution_convert_fusion.1 = bf16[768,2048]{1,0:T(8,128)(2,1)} fusion(bf16[1,512,2048]{2,1,0:T(8,128)(2,1)S(1)} %copy-done, f32[768,512]{1,0:T(8,128)} %fusion.52, bf16[768,2048]{1,0:T(8,128)(2,1)} %reshape.173, bf16[1,2048,512]{2,1,0:T(8,128)(2,1)} %param.39), kind=kOutput, calls=%fused_computation.52 | convolution fusion | flops 3225157632 | bytes 12058624 | tf_op jit(solution)/shard_map/dot_general | solution.py:185
  595.4 6.3 reshape.174
  601.7 26.4 %all-to-all-done.3 = bf16[128,6,2048]{2,1,0:T(8,128)(2,1)} async-done(((bf16[128,6,2048]{2,1,0:T(8,128)(2,1)}), bf16[128,6,2048]{2,1,0:T(8,128)(2,1)}, u32[]{:S(2)}, u32[]{:S(2)}) %all-to-all-start.3) | async-done | bytes 3145760 | tf_op jit(solution)/shard_map/all_to_all | solution.py:51
  628.1 5.5 all-to-all-start.2
  633.6 6.4 reshape.175
  640.0 5.5 fusion.50
  645.5 8.1 %convolution_convert_fusion = bf16[768,2048]{1,0:T(8,128)(2,1)} fusion(bf16[1,512,2048]{2,1,0:T(8,128)(2,1)S(1)} %copy-done, f32[768,512]{1,0:T(8,128)} %fusion.50, bf16[768,2048]{1,0:T(8,128)(2,1)} %reshape.175, bf16[1,2048,512]{2,1,0:T(8,128)(2,1)} %param.39), kind=kOutput, calls=%fused_computation.51 | convolution fusion | flops 3225157632 | bytes 12058624 | tf_op jit(solution)/shard_map/dot_general | solution.py:185
  653.7 6.3 reshape.176
  659.9 26.4 %all-to-all-done.2 = bf16[128,6,2048]{2,1,0:T(8,128)(2,1)} async-done(((bf16[128,6,2048]{2,1,0:T(8,128)(2,1)}), bf16[128,6,2048]{2,1,0:T(8,128)(2,1)}, u32[]{:S(2)}, u32[]{:S(2)}) %all-to-all-start.2) | async-done | bytes 3145760 | tf_op jit(solution)/shard_map/all_to_all | solution.py:254
  686.4 5.9 all-to-all-start.4
  692.5 3.2 fusion.193
  695.6 49.2 %all-to-all-done.4 = bf16[128,6,2048]{2,1,0:T(8,128)(2,1)} async-done(((bf16[128,6,2048]{2,1,0:T(8,128)(2,1)}), bf16[128,6,2048]{2,1,0:T(8,128)(2,1)}, u32[]{:S(2)}, u32[]{:S(2)}) %all-to-all-start.4) | async-done | bytes 3145760 | tf_op jit(solution)/shard_map/all_to_all | solution.py:254
  744.8 10.5 %pad_maximum_fusion = bf16[128,12,2048]{2,1,0:T(8,128)(2,1)} fusion(bf16[128,6,2048]{2,1,0:T(8,128)(2,1)} %all-to-all-done.4, bf16[128,6,2048]{2,1,0:T(8,128)(2,1)} %all-to-all-done.2), kind=kLoop, calls=%fused_computation.47 | loop fusion | flops 12582912 | bytes 12582912 | tf_op jit(solution)/shard_map/concatenate | solution.py:56
  755.4 10.7 %reshape.177 = bf16[1536,2048]{1,0:T(8,128)(2,1)} reshape(bf16[128,12,2048]{2,1,0:T(8,128)(2,1)} %pad_maximum_fusion) | data formatting | bytes 12582912 | tf_op jit(solution)/shard_map/reshape | solution.py:257
  766.1 12.4 %gather_fusion.1 = bf16[1024,2048]{1,0:T(8,128)(2,1)} fusion(bf16[1536,2048]{1,0:T(8,128)(2,1)} %reshape.177, s32[1024]{0:T(1024)S(1)} %broadcast_clamp_fusion), kind=kCustom, calls=%fused_computation.1 | custom fusion | bytes 8392704 | tf_op jit(solution)/shard_map/gather | solution.py:257
  778.5 7.2 reshape.178
  785.7 5.8 fusion.196
  791.6 5.8 fusion.35
  (292 shorter events, 149.6 us)
Async XLA Ops:
  6.5 580.7 %copy-start = (bf16[1,512,2048]{2,1,0:T(8,128)(2,1)S(1)}, bf16[1,512,2048]{2,1,0:T(8,128)(2,1)}, u32[]{:S(2)}) copy-start(bf16[1,512,2048]{2,1,0:T(8,128)(2,1)} %param.40) | copy-start | bytes 6291460
  6.5 260.9 %all-gather.13.cloned.1.call-start = ((), (), s32[]{:S(2)}) async-start(), calls=%async_computation.5 | async-start | bytes 1310720 | tf_op jit(solution)/shard_map/all_gather | solution.py:28
  14.8 4.7 copy-start.50
  19.5 163.8 %copy-start.45 = (bf16[512,512]{1,0:T(8,128)(2,1)S(1)}, bf16[512,512]{1,0:T(8,128)(2,1)}, u32[]{:S(2)}) copy-start(bf16[512,512]{1,0:T(8,128)(2,1)} %param.26) | copy-start | bytes 1572868
  187.1 2.3 copy-start.37
  191.7 2.1 copy-start.5
  241.3 26.1 %copy-start.52 = (f32[8,4]{1,0:T(8,128)}, f32[8,4]{1,0:T(8,128)S(1)}, u32[]{:S(2)}) copy-start(f32[8,4]{1,0:T(8,128)S(1)} %get-tuple-element.435) | copy-start | bytes 388
  242.1 51.5 %all-gather.19.cloned.1.call-start = ((), (), s32[]{:S(2)}) async-start(), calls=%async_computation.8 | async-start | bytes 1310720 | tf_op jit(solution)/shard_map/all_gather | solution.py:28
  242.8 81.3 %all-gather.21.cloned.1.call-start = ((), (), s32[]{:S(2)}) async-start(), calls=%async_computation.9 | async-start | bytes 1310720 | tf_op jit(solution)/shard_map/all_gather | solution.py:28
  267.4 29.9 %copy-start.4 = (f32[16,128,128]{2,1,0:T(8,128)S(1)}, f32[16,128,128]{2,1,0:T(8,128)}, u32[]{:S(2)}) copy-start(f32[16,128,128]{2,1,0:T(8,128)} %all-gather.13.cloned.1.call-done) | copy-start | bytes 3145732
  293.5 3.8 copy-start.43
  295.0 4.5 copy-start.21
  299.5 50.6 %all-gather.15.cloned.1.call-start = ((), (), s32[]{:S(2)}) async-start(), calls=%async_computation.6 | async-start | bytes 1310720 | tf_op jit(solution)/shard_map/all_gather | solution.py:28
  300.6 2.7 copy-start.48
  301.0 3.2 copy-start.14
  303.2 5.6 copy-start.46
  303.3 83.9 %all-gather.23.cloned.1.call-start = ((), (), s32[]{:S(2)}) async-start(), calls=%async_computation.10 | async-start | bytes 1310720 | tf_op jit(solution)/shard_map/all_gather | solution.py:28
  350.1 3.8 copy-start.3
  350.1 3.8 copy-start.42
  351.7 4.5 copy-start.25
  356.2 50.9 %all-gather.17.cloned.1.call-start = ((), (), s32[]{:S(2)}) async-start(), calls=%async_computation.7 | async-start | bytes 1310720 | tf_op jit(solution)/shard_map/all_gather | solution.py:28
  365.3 2.9 copy-start.12
  369.2 2.6 copy-start.53
  371.8 10.4 %copy-start.6 = (f32[8,64,4,128]{3,2,1,0:T(4,128)S(1)}, f32[8,64,4,128]{3,2,1,0:T(4,128)}, u32[]{:S(2)}) copy-start(f32[8,64,4,128]{3,2,1,0:T(4,128)} %reshape.171) | copy-start | bytes 3145732
  377.7 4.5 copy-start.13
  377.7 4.5 copy-start.39
  382.2 2.1 copy-start.15
  382.2 2.1 copy-start.17
  382.2 2.1 copy-start.20
  382.2 2.1 copy-start.24
  382.3 2.5 copy-start.26
  382.3 2.5 copy-start.28
  382.3 2.5 copy-start.34
  382.3 2.5 copy-start.36
  407.1 2.9 copy-start.7
  410.0 3.0 copy-start.38
  410.0 3.4 copy-start.22
  410.0 3.4 copy-start.27
  410.0 3.4 copy-start.30
  410.0 3.4 copy-start.32
  410.0 3.4 copy-start.44
  411.5 2.3 copy-start.8
  471.4 4.9 copy-start.49
  569.9 58.2 %all-to-all-start.3 = ((bf16[128,6,2048]{2,1,0:T(8,128)(2,1)}), bf16[128,6,2048]{2,1,0:T(8,128)(2,1)}, u32[]{:S(2)}, u32[]{:S(2)}) async-start(bf16[128,6,2048]{2,1,0:T(8,128)(2,1)} %get-tuple-element.230), calls=%async_computation.3 | async-start | bytes 8388608 | tf_op jit(solution)/shard_map/all_to_all | solution.py:51
  628.1 58.2 %all-to-all-start.2 = ((bf16[128,6,2048]{2,1,0:T(8,128)(2,1)}), bf16[128,6,2048]{2,1,0:T(8,128)(2,1)}, u32[]{:S(2)}, u32[]{:S(2)}) async-start(bf16[128,6,2048]{2,1,0:T(8,128)(2,1)} %reshape.174), calls=%async_computation.2 | async-start | bytes 8388608 | tf_op jit(solution)/shard_map/all_to_all | solution.py:254
  659.9 32.4 %copy-start.51 = (f32[256,4]{0,1:T(4,128)S(1)}, f32[256,4]{0,1:T(4,128)}, u32[]{:S(2)}) copy-start(f32[256,4]{0,1:T(4,128)} %param.37) | copy-start | bytes 12292
  659.9 32.6 %copy-start.41 = (bf16[256,2048]{1,0:T(8,128)(2,1)S(1)}, bf16[256,2048]{1,0:T(8,128)(2,1)}, u32[]{:S(2)}) copy-start(bf16[256,2048]{1,0:T(8,128)(2,1)} %copy-done.40) | copy-start | bytes 3145732
  686.4 58.5 %all-to-all-start.4 = ((bf16[128,6,2048]{2,1,0:T(8,128)(2,1)}), bf16[128,6,2048]{2,1,0:T(8,128)(2,1)}, u32[]{:S(2)}, u32[]{:S(2)}) async-start(bf16[128,6,2048]{2,1,0:T(8,128)(2,1)} %reshape.176), calls=%async_computation.4 | async-start | bytes 8388608 | tf_op jit(solution)/shard_map/all_to_all | solution.py:254
  (15 other events, 14.3 us)
Sparse Core Ops, SparseCore 0:
  242.2 25.1 all-gather.12
  269.1 24.4 all-gather.18
  299.6 24.4 all-gather.20
  325.7 24.4 all-gather.14
  356.3 24.6 all-gather.22
  382.5 24.5 all-gather.16
where the time goes:
time: 816 us; the launch traced here: 805 us
  waiting for transfers between devices  213 us (26%)
  other arithmetic  199 us (24%)
  matrix products  161 us (20%)
  local copies, waits for them, and re-layouts  131 us (16%)
  blocking collectives  67.7 us (8%)
  starting transfers between devices  17.6 us (2%)
  between operations  14.8 us (2%)
    another operation x4, other arithmetic, block_terms(): jax.scipy.linalg.solve_triangular(lower, right, lower=True, unit_diagonal...  159 us
    all_gather x6, waiting for transfers between devices, entering(): pieces = jax.tree.map(lambda part: lax.all_gather(part, axis), running)  110 us
    all_to_all x2, waiting for transfers between devices, serve(): lax.all_to_all(expert_ffn(arrived), SP_TP, split_axis=0, concat_axis=0, t...  75.6 us
    all_to_all x1, blocking collectives, items_in_groups(): lax.all_to_all(group, axis, split_axis=split_dim, concat_axis=concat_dim,...  61 us
    all_to_all x1, waiting for transfers between devices, items_in_groups(): lax.all_to_all(group, axis, split_axis=split_dim, concat_axis=concat_dim,...  26.4 us
    dot_general x3, matrix products, feed_forward(): return jnp.dot(hidden, w_down, preferred_element_type=jnp.float32)  22.1 us
    reshape x2, local copies, waits for them, and re-layouts, shards(): back.reshape(experts * room, -1)[target].reshape(length, TOP_K, -1)  17.9 us
    gather x2, local copies, waits for them, and re-layouts, shards(): normed[source]  17.7 us
  transfers between devices with their start and end apart: 9, of which 8 were waited for; matrix products, arithmetic and copies ran while one was open for 12% of the time, Pallas kernels for 0%

commit v1 on v0

v1 whole, which is shorter than its diff:
```python
import functools

import jax
import jax.numpy as jnp
from jax import lax
from jax.experimental import pallas as pl
from jax.experimental.pallas import tpu as pltpu
from jax.sharding import Mesh
from jax.sharding import PartitionSpec as P

TOP_K = 4
SPAN = 64
CAP = 12
HD = 128
AXES = ("sp_0", "sp_1", "sp_2", "tp")
SP = AXES[:3]
EPS = 1e-06
F32, BF16 = jnp.float32, jnp.bfloat16
HIGH = lax.Precision.HIGHEST
MESH = pl.DeviceIdType.MESH
VMEM = pl.BlockSpec(memory_space=pltpu.VMEM)
OFFSETS = (1, 3, 2)
ORDERS = ((2, 1, 0), (1, 0, 2), (0, 2, 1))
STATE_TYPE = BF16


def params(**kw):
    return pltpu.CompilerParams(vmem_limit_bytes=62 * 2**20, **kw)


def mm(a, b, dims=((1,), (0,))):
    return lax.dot_general(a, b, (dims, ((), ())), preferred_element_type=F32)


def halves(x):
    high = x.astype(BF16)
    return high, (x - high.astype(F32)).astype(BF16)


def mm3(a, b, dims=((1,), (0,))):
    (ah, al), (bh, bl) = a, b
    return mm(ah, bh, dims) + mm(al, bh, dims) + mm(ah, bl, dims)


def silu(x):
    return x / (1.0 + jnp.exp(-x))


def iota(shape, dim):
    return lax.broadcasted_iota(jnp.int32, shape, dim)


def local_kernel(
    q_ref, k_ref, v_ref, beta_ref, decay_ref, decay_t_ref,
    map_ref, z_ref, h_ref,
    low_s, score_s, inv_s, right_s, qd_s, kdt_s, wu_s, qp_s, step_s, pre_s,
):
    heads, tokens = 4, q_ref.shape[0]
    blocks = tokens // SPAN
    i256, j256 = iota((256, 256), 0), iota((256, 256), 1)
    same = (i256 // SPAN) == (j256 // SPAN)
    tri = jnp.where(same & (j256 <= i256), 1.0, 0.0)
    tri_t = jnp.where(same & (i256 <= j256), 1.0, 0.0)
    ones = jnp.where(same, 1.0, 0.0)

    def high(a, b):
        return lax.dot_general(a, b, (((1,), (0,)), ((), ())), precision=HIGH, preferred_element_type=F32)

    dec = [decay_ref[256 * i : 256 * i + 256, :] for i in range(2)]
    dec_t = [decay_t_ref[:, 256 * i : 256 * i + 256] for i in range(2)]
    g_col = jnp.concatenate([high(tri, d) for d in dec], 0)
    total_col = jnp.concatenate([high(ones, d) for d in dec], 0)
    g_row = jnp.concatenate([high(d, tri_t) for d in dec_t], 1)
    total_row = jnp.concatenate([high(d, ones) for d in dec_t], 1)
    beta = beta_ref[...]

    row, lane = iota((SPAN, 128), 0), iota((SPAN, 128), 1)
    first = lane < SPAN
    place = lane % SPAN
    causal, strict = row >= place, row > place
    pair_masks = [jnp.where(first, 1.0, 0.0).astype(BF16), jnp.where(first, 0.0, 1.0).astype(BF16)]
    first_wide = iota((128, 128), 1) < SPAN
    eye = jnp.where(iota((128, 128), 0) == iota((128, 128), 1), 1.0, 0.0)

    for h in range(heads):
        cols = slice(h * HD, h * HD + HD)
        q = silu(q_ref[:, cols].astype(F32))
        q = q * lax.rsqrt(jnp.sum(q * q, axis=-1, keepdims=True) + EPS)
        k = silu(k_ref[:, cols].astype(F32))
        k = k * lax.rsqrt(jnp.sum(k * k, axis=-1, keepdims=True) + EPS)
        v = silu(v_ref[:, cols].astype(F32))
        b_h, g_h = beta[:, h : h + 1], g_col[:, h : h + 1]
        grown = jnp.exp(g_h)
        kb = k * b_h
        right_s[h, :, :HD] = kb * grown
        right_s[h, :, HD:] = v * b_h
        qd_s[h] = q * grown
        gr = g_row[h : h + 1, :]
        kdt_s[h] = k.T * jnp.exp(total_row[h : h + 1, :] - gr)
        ks, kbs, qs = halves(k), halves(kb), halves(q)
        for j in range(tokens // 128):
            rows = slice(128 * j, 128 * j + 128)
            left = tuple(jnp.concatenate([a[rows], b[rows]], 0) for a, b in zip(kbs, qs))
            both = mm3(left, tuple(a[rows] for a in ks), ((1,), (1,)))
            inner = jnp.where(first, both[0:64], both[64:128])
            score = jnp.where(first, both[128:192], both[192:256])
            gi = jnp.where(first, g_h[128 * j : 128 * j + 64], g_h[128 * j + 64 : 128 * j + 128])
            spread = jnp.where(causal, gi - gr[:, rows], 0.0)
            decay = jnp.where(causal, jnp.exp(spread), 0.0)
            low_s[h, :, rows] = jnp.where(strict, inner * decay, 0.0)
            score_s[h, :, rows] = score * decay

    r4, l4 = iota((SPAN, 256), 0), iota((SPAN, 256), 1)
    p4 = l4 % SPAN
    quad_masks = [jnp.where(l4 // SPAN == n, 1.0, 0.0).astype(BF16) for n in range(4)]
    eye4 = jnp.where(r4 == p4, 1.0, 0.0)

    def diag4(x):
        return jnp.concatenate([x * m for m in quad_masks], 0)

    def times(a, b):
        return mm3(a, tuple(diag4(x) for x in b))

    groups = [(h, slice(256 * i, 256 * i + 256)) for h in range(heads) for i in range(2)]
    for part in range(2):
        mine = groups[4 * part : 4 * part + 4]
        lows = [low_s[h, :, s] for h, s in mine]
        small = r4 // 8 == p4 // 8
        d1 = [jnp.where(small, x, 0.0) for x in lows]
        d1s = [halves(x) for x in d1]
        d2s = [halves(times(x, x)) for x in d1s]
        x1 = [eye4 - x for x in d1]
        x2 = [x + times(halves(x), d) for x, d in zip(x1, d2s)]
        d4s = [halves(times(d, d)) for d in d2s]
        inv = [x + times(halves(x), d) for x, d in zip(x2, d4s)]
        for size in (8, 16, 32):
            off = (r4 // (2 * size) == p4 // (2 * size)) & (r4 // size != p4 // size)
            invs = [halves(x) for x in inv]
            ex = [halves(times(halves(jnp.where(off, x, 0.0)), y)) for x, y in zip(lows, invs)]
            inv = [x - times(y, e) for x, y, e in zip(inv, invs, ex)]
        for (h, s), x in zip(mine, inv):
            inv_s[h, :, s] = x

    def diag2(x):
        return jnp.concatenate([x * m for m in pair_masks], 0)

    for h in range(heads):
        for j in range(tokens // 128):
            rows = slice(128 * j, 128 * j + 128)
            inv = tuple(diag2(x) for x in halves(inv_s[h, :, rows]))
            wu = mm3(inv, halves(right_s[h, rows, :]))
            wus = halves(wu)
            score = tuple(diag2(x) for x in halves(score_s[h, :, rows]))
            applied = mm3(score, wus)
            qp_s[h, rows, :] = qd_s[h, rows, :] - applied[:, :HD]
            h_ref[h, rows, :] = applied[:, HD:]
            kdt = kdt_s[h, :, rows]
            kdt = jnp.concatenate([jnp.where(first_wide, kdt, 0.0), jnp.where(first_wide, 0.0, kdt)], 0)
            change = mm3(halves(kdt), wus)
            for c in range(2):
                n = 2 * j + c
                factor = jnp.exp(total_col[n * SPAN : n * SPAN + 1, h : h + 1])
                step_s[h, n, :, :HD] = eye * factor - change[128 * c : 128 * c + 128, :HD]
                step_s[h, n, :, HD:] = change[128 * c : 128 * c + 128, HD:]

    for h in range(heads):
        pre_s[h, 1] = step_s[h, 0]
    for n in range(1, blocks):
        for h in range(heads):
            moved = mm3(halves(step_s[h, n, :, :HD]), halves(pre_s[h, n]))
            pre = jnp.concatenate([moved[:, :HD], moved[:, HD:] + step_s[h, n, :, HD:]], 1)
            if n + 1 < blocks:
                pre_s[h, n + 1] = pre
            else:
                map_ref[h] = pre.astype(map_ref.dtype)
    for h in range(heads):
        z_ref[h, 0:SPAN, :] = qp_s[h, 0:SPAN, :]
        for n in range(1, blocks):
            rows = slice(SPAN * n, SPAN * n + SPAN)
            moved = mm3(halves(qp_s[h, rows, :]), halves(pre_s[h, n]))
            z_ref[h, rows, :] = moved[:, :HD]
            h_ref[h, rows, :] = h_ref[h, rows, :] + moved[:, HD:]


def local_terms(q, k, v, beta, decay):
    tokens = q.shape[0]
    heads = 4
    return pl.pallas_call(
        local_kernel,
        out_shape=(
            jax.ShapeDtypeStruct((heads, HD, 2 * HD), STATE_TYPE),
            jax.ShapeDtypeStruct((heads, tokens, HD), F32),
            jax.ShapeDtypeStruct((heads, tokens, HD), F32),
        ),
        in_specs=[VMEM] * 6,
        out_specs=(VMEM,) * 3,
        scratch_shapes=[
            pltpu.VMEM((heads, SPAN, tokens), F32),
            pltpu.VMEM((heads, SPAN, tokens), F32),
            pltpu.VMEM((heads, SPAN, tokens), F32),
            pltpu.VMEM((heads, tokens, 2 * HD), F32),
            pltpu.VMEM((heads, tokens, HD), F32),
            pltpu.VMEM((heads, HD, tokens), F32),
            pltpu.VMEM((8, 128), F32),
            pltpu.VMEM((heads, tokens, HD), F32),
            pltpu.VMEM((heads, tokens // SPAN, HD, 2 * HD), F32),
            pltpu.VMEM((heads, tokens // SPAN, HD, 2 * HD), F32),
        ],
        compiler_params=params(),
        name="local_terms",
    )(q, k, v, beta, decay, decay.T)


def along(dim, off):
    at = [lax.axis_index(a) for a in AXES]
    at[dim] = lax.rem(at[dim] + off, 4)
    return tuple(at)


def partner():
    at = [lax.axis_index(a) for a in AXES]
    at[3] = 1 - at[3]
    return tuple(at)


def greet(dims, pair):
    barrier = pltpu.get_barrier_semaphore()
    count = 0
    for dim in dims:
        for off in OFFSETS:
            pl.semaphore_signal(barrier, inc=1, device_id=along(dim, off), device_id_type=MESH)
            count += 1
    if pair:
        pl.semaphore_signal(barrier, inc=1, device_id=partner(), device_id_type=MESH)
        count += 1
    pl.semaphore_wait(barrier, count)


def mixed_kernel(
    map_ref, z_ref, h_ref, gate_ref, gain_ref, out_w_ref, residual_ref, norm_ref,
    attended_ref, normed_ref,
    row_s, plane_s, all_s, row_total, plane_total, state_out, state_in, mix_s, mix_in, acc_s,
    send_sem, recv_sem,
):
    greet((0, 1, 2), True)
    z, y, x, c = (lax.axis_index(a) for a in AXES)

    def send(stage, dim, source, target):
        copies = []
        here = lax.axis_index(AXES[dim])
        for n, off in enumerate(OFFSETS):
            copies.append(
                pltpu.make_async_remote_copy(
                    src_ref=source(lax.rem(here + off, 4)),
                    dst_ref=target.at[here],
                    send_sem=send_sem.at[stage, n],
                    recv_sem=recv_sem.at[stage, n],
                    device_id=along(dim, off),
                    device_id_type=MESH,
                )
            )
        for copy in copies:
            copy.start()
        return copies

    def applied(step, carried):
        high, low = halves(carried)
        moved = mm(step[:, :HD], high) + mm(step[:, :HD], low)
        if carried.shape[1] == HD:
            return moved + step[:, HD:].astype(F32)
        return jnp.concatenate([moved[:, :HD], moved[:, HD:] + step[:, HD:].astype(F32)], 1)

    def total(steps):
        carried = steps[0].astype(F32)
        for i in range(1, 4):
            carried = applied(steps[i], carried)
        return carried.astype(STATE_TYPE)

    sent = []
    copies = send(0, 2, lambda t: map_ref.at[t], row_s)
    row_s[x] = map_ref[x]
    for copy in copies:
        copy.wait_recv()
    sent += copies
    row_total[...] = total(row_s)
    copies = send(1, 1, lambda t: row_total, plane_s)
    plane_s[y] = row_total[...]
    for copy in copies:
        copy.wait_recv()
    sent += copies
    plane_total[...] = total(plane_s)
    copies = send(2, 0, lambda t: plane_total, all_s)
    all_s[z] = plane_total[...]
    for copy in copies:
        copy.wait_recv()
    sent += copies
    state = jnp.where(z > 0, all_s[0, :, HD:].astype(F32), 0.0)
    for i in range(1, 3):
        state = jnp.where(i < z, applied(all_s[i], state), state)
    for i in range(3):
        state = jnp.where(i < y, applied(plane_s[i], state), state)
    state_out[0] = state.astype(STATE_TYPE)
    for i in range(3):
        state = applied(row_s[i], state)
        state_out[i + 1] = state.astype(STATE_TYPE)
    copies = send(3, 2, lambda t: state_out.at[t], state_in)
    state_in[x] = state_out[x]
    for copy in copies:
        copy.wait_recv()
    sent += copies

    gain = gain_ref[...]
    for h in range(4):
        high, low = halves(z_ref[h])
        state = state_in[h]
        mix = h_ref[h] + mm(high, state) + mm(low, state)
        mix = mix * lax.rsqrt(jnp.mean(mix * mix, axis=-1, keepdims=True) + EPS) * gain
        mix = mix * silu(gate_ref[:, h * HD : h * HD + HD].astype(F32))
        mix_s[:, h * HD : h * HD + HD] = mix.astype(BF16)
    half = mix_s.shape[0] // 2
    width = mix_s.shape[1]
    other = 1 - c
    swap = pltpu.make_async_remote_copy(
        src_ref=mix_s.at[pl.ds(pl.multiple_of(other * half, half), half)],
        dst_ref=mix_in,
        send_sem=send_sem.at[4, 0],
        recv_sem=recv_sem.at[4, 0],
        device_id=partner(),
        device_id_type=MESH,
    )
    swap.start()
    own = pl.ds(pl.multiple_of(c * half, half), half)
    own_w = pl.ds(pl.multiple_of(c * width, width), width)
    other_w = pl.ds(pl.multiple_of(other * width, width), width)
    model = out_w_ref.shape[1]
    for n in range(model // 512):
        cols = slice(512 * n, 512 * n + 512)
        acc_s[:, cols] = residual_ref[:, cols].astype(F32) + mm(mix_s[own, :], out_w_ref[own_w, cols])
    swap.wait()
    squares = jnp.zeros((half, 1), F32)
    for n in range(model // 512):
        cols = slice(512 * n, 512 * n + 512)
        piece = acc_s[:, cols] + mm(mix_in[...], out_w_ref[other_w, cols])
        piece = piece.astype(BF16)
        attended_ref[:, cols] = piece
        wide = piece.astype(F32)
        acc_s[:, cols] = wide
        squares = squares + jnp.sum(wide * wide, axis=-1, keepdims=True)
    scale = lax.rsqrt(squares / model + EPS)
    for n in range(model // 512):
        cols = slice(512 * n, 512 * n + 512)
        normed_ref[own, cols] = (acc_s[:, cols] * scale * norm_ref[:, cols]).astype(BF16)
    share = pltpu.make_async_remote_copy(
        src_ref=normed_ref.at[own],
        dst_ref=normed_ref.at[own],
        send_sem=send_sem.at[4, 1],
        recv_sem=recv_sem.at[4, 1],
        device_id=partner(),
        device_id_type=MESH,
    )
    share.start()
    share.wait()
    for copy in sent:
        copy.wait_send()


def mixed(maps, z, h, gate, gain, out_w, residual, norm_gain):
    half, model = residual.shape
    return pl.pallas_call(
        mixed_kernel,
        out_shape=(
            jax.ShapeDtypeStruct((half, model), BF16),
            jax.ShapeDtypeStruct((2 * half, model), BF16),
        ),
        in_specs=[VMEM] * 8,
        out_specs=(VMEM,) * 2,
        scratch_shapes=[
            pltpu.VMEM((4, HD, 2 * HD), STATE_TYPE),
            pltpu.VMEM((4, HD, 2 * HD), STATE_TYPE),
            pltpu.VMEM((4, HD, 2 * HD), STATE_TYPE),
            pltpu.VMEM((HD, 2 * HD), STATE_TYPE),
            pltpu.VMEM((HD, 2 * HD), STATE_TYPE),
            pltpu.VMEM((4, HD, HD), STATE_TYPE),
            pltpu.VMEM((4, HD, HD), STATE_TYPE),
            pltpu.VMEM((2 * half, 4 * HD), BF16),
            pltpu.VMEM((half, 4 * HD), BF16),
            pltpu.VMEM((half, model), F32),
            pltpu.SemaphoreType.DMA((5, 3)),
            pltpu.SemaphoreType.DMA((5, 3)),
        ],
        compiler_params=params(collective_id=0, has_side_effects=True),
        name="mixed",
    )(maps, z, h, gate, gain, out_w, residual, norm_gain)


def piece(ref, dim, i):
    if dim == 0:
        return ref.at[i]
    if dim == 1:
        return ref.at[:, i]
    return ref.at[:, :, i]


def exchange_kernel(src_ref, dst_ref, one_ref, two_ref, send_sem, recv_sem):
    greet((0, 1, 2), False)
    buffers = (src_ref, one_ref, two_ref, dst_ref)
    sent = []
    for stage in range(3):
        copies = []
        for n, off in enumerate(OFFSETS):
            for k in range(3):
                dim = ORDERS[k][stage]
                here = lax.axis_index(AXES[dim])
                copy = pltpu.make_async_remote_copy(
                    src_ref=piece(buffers[stage].at[k], dim, lax.rem(here + off, 4)),
                    dst_ref=piece(buffers[stage + 1].at[k], dim, here),
                    send_sem=send_sem.at[stage, k, n],
                    recv_sem=recv_sem.at[stage, k, n],
                    device_id=along(dim, off),
                    device_id_type=MESH,
                )
                copy.start()
                copies.append(copy)
        for k in range(3):
            dim = ORDERS[k][stage]
            here = lax.axis_index(AXES[dim])
            source = piece(buffers[stage].at[k], dim, here)
            target = piece(buffers[stage + 1].at[k], dim, here)

            def keep(i, _):
                target[i // 4, i % 4] = source[i // 4, i % 4]
                return 0

            lax.fori_loop(0, 16, keep, 0)
        for copy in copies:
            copy.wait_recv()
        sent += copies
    for copy in sent:
        copy.wait_send()


def exchange(rows):
    return pl.pallas_call(
        exchange_kernel,
        out_shape=jax.ShapeDtypeStruct(rows.shape, rows.dtype),
        in_specs=[VMEM],
        out_specs=VMEM,
        scratch_shapes=[pltpu.VMEM(rows.shape, rows.dtype)] * 2
        + [pltpu.SemaphoreType.DMA((3, 3, 3))] * 2,
        compiler_params=params(collective_id=1, has_side_effects=True),
        name="exchange",
    )(rows)


def dispatch_kernel(normed_ref, ids_ref, expert_ref, rows_ref, code_s):
    tokens = normed_ref.shape[0]
    half = tokens // 2
    chips = expert_ref.shape[0]
    chosen = jnp.zeros((chips, tokens), F32)
    for j in range(TOP_K):
        chosen = chosen + jnp.where(ids_ref[j : j + 1, :] == expert_ref[...], 1.0, 0.0)
    i, j = iota((tokens, tokens), 0), iota((tokens, tokens), 1)
    before = jnp.where((i // half == j // half) & (i < j), 1.0, 0.0).astype(BF16)
    slot = mm(chosen.astype(BF16), before)
    shift = jnp.where(iota((chips, tokens), 1) < half, 0.0, float(CAP))
    code_s[...] = jnp.where(chosen > 0.0, slot + shift, -1.0)
    for k in range(3):
        low = 0 if k < 2 else half
        high = half if k == 0 else tokens

        def one(zi, _):
            code = code_s[pl.ds(pl.multiple_of(zi * 16, 16), 16), low:high]
            wanted = (iota((16, 8, high - low), 1) + 8 * k).astype(F32)
            pick = jnp.where(code[:, None, :] == wanted, 1.0, 0.0).reshape(128, high - low).astype(BF16)
            rows = mm(pick, normed_ref[low:high, :]).astype(BF16)
            rows_ref[k, zi] = rows.reshape(4, 4, 8, rows.shape[-1])
            return 0

        lax.fori_loop(0, 4, one, 0)


def dispatch(normed, ids, experts):
    return pl.pallas_call(
        dispatch_kernel,
        out_shape=jax.ShapeDtypeStruct((3, 4, 4, 4, 8, normed.shape[1]), BF16),
        in_specs=[VMEM] * 3,
        out_specs=VMEM,
        scratch_shapes=[pltpu.VMEM((64, normed.shape[0]), F32)],
        compiler_params=params(),
        name="dispatch",
    )(normed, ids, experts)


def experts_kernel(rows_ref, gate_ref, up_ref, down_ref, out_ref):
    def one(k, _):
        rows = rows_ref[k].reshape(512, rows_ref.shape[-1])
        hidden = silu(mm(rows, gate_ref[...])) * mm(rows, up_ref[...])
        result = mm(hidden.astype(BF16), down_ref[...]).astype(BF16)
        out_ref[k] = result.reshape(out_ref.shape[1:])
        return 0

    lax.fori_loop(0, 3, one, 0)


def run_experts(rows, gate, up, down):
    return pl.pallas_call(
        experts_kernel,
        out_shape=jax.ShapeDtypeStruct(rows.shape, BF16),
        in_specs=[VMEM] * 4,
        out_specs=VMEM,
        compiler_params=params(),
        name="experts",
    )(rows, gate, up, down)


def combine_kernel(
    back_ref, ids_ref, expert_ref, weight_ref, normed_ref, attended_ref, gate_ref, up_ref, down_ref,
    out_ref, pick_s, away_s, here_s, send_sem, recv_sem,
):
    greet((), True)
    tokens, model = normed_ref.shape
    half = tokens // 2
    chips = expert_ref.shape[1]
    c = lax.axis_index("tp")
    chosen = jnp.zeros((tokens, chips), F32)
    weight = jnp.zeros((tokens, chips), F32)
    for j in range(TOP_K):
        hit = ids_ref[:, j : j + 1] == expert_ref[...]
        chosen = chosen + jnp.where(hit, 1.0, 0.0)
        weight = weight + jnp.where(hit, weight_ref[:, j : j + 1], 0.0)
    i, j = iota((tokens, tokens), 0), iota((tokens, tokens), 1)
    before = jnp.where((i // half == j // half) & (j < i), 1.0, 0.0).astype(BF16)
    slot = mm(before, chosen.astype(BF16))
    shift = jnp.where(iota((tokens, chips), 0) < half, 0.0, float(CAP))
    code = jnp.where(chosen > 0.0, slot + shift, -1.0).astype(BF16)
    spread = jnp.where(iota((chips, 8 * chips), 1) // 8 == iota((chips, 8 * chips), 0), 1.0, 0.0).astype(BF16)
    code = mm(code, spread)
    weight = mm(weight.astype(BF16), spread)
    place = (iota((tokens, 8 * chips), 1) % 8).astype(F32)
    for k in range(3):
        pick_s[k] = jnp.where(code == place + 8.0 * k, weight, 0.0).astype(BF16)

    def partial(core, n):
        rows = pl.ds(pl.multiple_of(core * half, half), half)
        cols = slice(512 * n, 512 * n + 512)
        total = jnp.zeros((half, 512), F32)
        for k in range(3):
            total = total + mm(pick_s[k, rows, :], back_ref[k, :, :, :, :, cols].reshape(8 * chips, 512))
        return total

    for n in range(model // 512):
        away_s[:, 512 * n : 512 * n + 512] = partial(1 - c, n)
    copy = pltpu.make_async_remote_copy(
        src_ref=away_s,
        dst_ref=here_s,
        send_sem=send_sem,
        recv_sem=recv_sem,
        device_id=partner(),
        device_id_type=MESH,
    )
    copy.start()
    own = pl.ds(pl.multiple_of(c * half, half), half)
    rows = normed_ref[own, :]
    hidden = (silu(mm(rows, gate_ref[...])) * mm(rows, up_ref[...])).astype(BF16)
    copy.wait()
    for n in range(model // 512):
        cols = slice(512 * n, 512 * n + 512)
        total = attended_ref[:, cols].astype(F32) + mm(hidden, down_ref[:, cols])
        out_ref[:, cols] = (total + (partial(c, n) + here_s[:, cols])).astype(BF16)


def combine(back, ids, experts, weight, normed, attended, gate, up, down):
    half, model = attended.shape
    return pl.pallas_call(
        combine_kernel,
        out_shape=jax.ShapeDtypeStruct((half, model), BF16),
        in_specs=[VMEM] * 9,
        out_specs=VMEM,
        scratch_shapes=[
            pltpu.VMEM((3, 2 * half, 512), BF16),
            pltpu.VMEM((half, model), F32),
            pltpu.VMEM((half, model), F32),
            pltpu.SemaphoreType.DMA,
            pltpu.SemaphoreType.DMA,
        ],
        compiler_params=params(collective_id=2, has_side_effects=True),
        name="combine",
    )(back, ids, experts, weight, normed, attended, gate, up, down)


def shards(
    projected_queries,
    projected_keys,
    projected_values,
    output_gate_values,
    write_strength_logits,
    decay_input_logits,
    head_rate_logarithm,
    extra_log_decay,
    per_head_norm_gain,
    output_matrix,
    residual,
    mixture_norm_gain,
    selected_expert_index,
    routing_weight,
    routed_gate_weight,
    routed_up_weight,
    routed_down_weight,
    common_gate_weight,
    common_up_weight,
    common_down_weight,
):
    beta = jax.nn.sigmoid(write_strength_logits.astype(F32))
    decay = extra_log_decay - jnp.exp(head_rate_logarithm)[None, :] * jax.nn.softplus(
        decay_input_logits.astype(F32) - 6.0
    )
    ids = lax.all_gather(selected_expert_index, "tp", tiled=True)
    weight = lax.all_gather(routing_weight, "tp", tiled=True)
    experts = 2 * jnp.arange(64, dtype=jnp.int32) + lax.axis_index("tp").astype(jnp.int32)
    maps, z, h = local_terms(projected_queries, projected_keys, projected_values, beta, decay)
    attended, normed = mixed(
        maps,
        z,
        h,
        output_gate_values,
        per_head_norm_gain[None, :],
        output_matrix,
        residual,
        mixture_norm_gain[None, :],
    )
    outgoing = dispatch(normed, ids.T, experts[:, None])
    arrived = exchange(outgoing)
    served = run_experts(arrived, routed_gate_weight[0], routed_up_weight[0], routed_down_weight[0])
    back = exchange(served)
    return combine(
        back,
        ids,
        experts[None, :],
        weight,
        normed,
        attended,
        common_gate_weight,
        common_up_weight,
        common_down_weight,
    )


def solution(mesh):
    finer = Mesh(mesh.devices.reshape(4, 4, 4, mesh.shape["tp"]), AXES)
    in_specs = (
        P(SP, "tp"),
        P(SP, "tp"),
        P(SP, "tp"),
        P(SP, "tp"),
        P(SP, "tp"),
        P(SP, "tp"),
        P("tp"),
        P(SP, "tp"),
        P(),
        P(),
        P(AXES, None),
        P(),
        P(AXES, None),
        P(AXES, None),
        P(AXES, None, None),
        P(AXES, None, None),
        P(AXES, None, None),
        P(),
        P(),
        P(),
    )
    return jax.shard_map(
        shards, mesh=finer, in_specs=in_specs, out_specs=P(AXES, None), check_vma=False
    )
```

time: 816 us -> 272 us (0.33); the launches traced: 805 us -> 271 us
  Pallas kernels: 0 us -> 255 us
  waiting for transfers between devices: 213 us -> 0 us
  other arithmetic: 199 us -> 2.67 us
  matrix products: 161 us -> 0 us
  local copies, waits for them, and re-layouts: 131 us -> 5.64 us
  blocking collectives: 67.7 us -> 7.76 us
  starting transfers between devices: 17.6 us -> 0 us
  between operations: 14.8 us -> 0.07 us
    pallas_call x0 -> x7, Pallas kernels: none -> 255 us  [the longest x2 153 us: exchange(): pl.pallas_call(exchange_kernel, out_shape=jax.ShapeDtypeStruct(rows.shape...]
    another operation x5 -> x0, other arithmetic: 160 us -> none  [the longest x4 159 us: block_terms(): jax.scipy.linalg.solve_triangular(lower, right, lower=True, unit_diagonal...]
    dot_general x100 -> x0, matrix products: 159 us -> none  [the longest x3 22.1 us: feed_forward(): return jnp.dot(hidden, w_down, preferred_element_type=jnp.float32)]
    all_gather x6 -> x0, waiting for transfers between devices: 110 us -> none  [entering(): pieces = jax.tree.map(lambda part: lax.all_gather(part, axis), running)]
    all_to_all x3 -> x0, waiting for transfers between devices: 102 us -> none  [the longest x2 75.6 us: serve(): lax.all_to_all(expert_ffn(arrived), SP_TP, split_axis=0, concat_axis=0, t...]
    all_to_all x2 -> x0, blocking collectives: 67.7 us -> none  [the longest x1 61 us: items_in_groups(): lax.all_to_all(group, axis, split_axis=split_dim, concat_axis=concat_dim,...]
    reshape x8 -> x0, local copies, waits for them, and re-layouts: 48.3 us -> none  [the longest x2 17.9 us: shards(): back.reshape(experts * room, -1)[target].reshape(length, TOP_K, -1)]
    gather x3 -> x0, local copies, waits for them, and re-layouts: 30.1 us -> none  [the longest x2 17.7 us: shards(): normed[source]]
  transfers between devices with their start and end apart: 9 -> 0, of which waited for: 8 -> 0; matrix products, arithmetic and copies ran while one was open for 12% -> 0% of each run, Pallas kernels for 0% -> 0%
where the time goes in v1:
time: 272 us; the launch traced here: 271 us
  Pallas kernels  255 us (94%)
  blocking collectives  7.76 us (3%)
  local copies, waits for them, and re-layouts  5.64 us (2%)
    pallas_call x2, Pallas kernels, exchange(): pl.pallas_call(exchange_kernel, out_shape=jax.ShapeDtypeStruct(rows.shape...  153 us
    pallas_call x1, Pallas kernels, mixed(): pl.pallas_call(mixed_kernel, out_shape=(jax.ShapeDtypeStruct((half, model...  39.5 us
    pallas_call x1, Pallas kernels, local_terms(): pl.pallas_call(local_kernel, out_shape=(jax.ShapeDtypeStruct((heads, HD,...  20.1 us
    pallas_call x1, Pallas kernels, run_experts(): pl.pallas_call(experts_kernel, out_shape=jax.ShapeDtypeStruct(rows.shape,...  17.6 us
    pallas_call x1, Pallas kernels, combine(): pl.pallas_call(combine_kernel, out_shape=jax.ShapeDtypeStruct((half, mode...  16.2 us
    pallas_call x1, Pallas kernels, dispatch(): pl.pallas_call(dispatch_kernel, out_shape=jax.ShapeDtypeStruct((3, 4, 4,...  8.87 us
    all_gather x1, blocking collectives, shards(): weight = lax.all_gather(routing_weight, 'tp', tiled=True)  5.76 us

profile of v1, /device:TPU:1, one launch (start us, length us, event | category | flops | bytes accessed | tf_op | source)
XLA Modules:
  0.0 271.5 jit_solution(12899672756367766512)
XLA Ops:
  0.0 0.7 exp.11
  0.7 0.8 fusion.1
  1.4 0.0 copy-start.1
  1.4 0.9 copy.29.decay_ref
  2.3 0.8 copy.26
  3.1 0.8 add_divide_fusion.beta_ref
  3.9 0.0 copy-done.1
  3.9 20.1 %local_terms.1 = (bf16[4,128,256]{2,1,0:T(8,128)(2,1)}, f32[4,512,128]{2,1,0:T(8,128)}, f32[4,512,128]{2,1,0:T(8,128)}) custom-call(bf16[512,512]{1,0:T(8,128)(2,1)} %q_ref.1, bf16[512,512]{1,0:T(8,128)(2,1)} %k_ref.1, bf16[512,512]{1,0:T(8,128)(2,1)} %v_ref.1, f32[512,4]{1,0:T(8,128)} %add_divide_fusion.beta_ref, f32[512,4]{1,0:T(8,128)} %copy.29.decay_ref, ...), custom_call_target="tpu_custom_call" | custom-call | tf_op jit(solution)/shard_map/local_terms/pallas_call | solution.py:188
  24.0 0.0 copy-start.2
  24.0 39.5 %mixed.1 = (bf16[256,2048]{1,0:T(8,128)(2,1)}, bf16[512,2048]{1,0:T(8,128)(2,1)}) custom-call(bf16[4,128,256]{2,1,0:T(8,128)(2,1)} %get-tuple-element.10.map_ref, f32[4,512,128]{2,1,0:T(8,128)} %get-tuple-element.11.z_ref, f32[4,512,128]{2,1,0:T(8,128)} %get-tuple-element.12.h_ref, bf16[512,512]{1,0:T(8,128)(2,1)} %gate_ref.2, f32[1,128]{1,0:T(1,128)} %bitcast.13, ...), custom_call_target="tpu_custom_call" | custom-call | tf_op jit(solution)/shard_map/mixed/pallas_call | solution.py:369
  63.5 0.0 copy-done.2
  63.5 0.1 copy.30
  63.7 2.0 all_gather.6.ids_ref
  65.7 0.0 copy-start
  65.7 0.7 copy.31.ids_ref
  66.4 0.6 multiply_add_fusion.expert_ref
  67.0 8.9 %dispatch.1.src_ref = bf16[3,4,4,4,8,2048]{5,4,3,2,1,0:T(8,128)(2,1)} custom-call(bf16[512,2048]{1,0:T(8,128)(2,1)} %get-tuple-element.13.normed_ref, s32[4,512]{1,0:T(4,128)} %copy.31.ids_ref, s32[64,1]{1,0:T(8,128)} %multiply_add_fusion.expert_ref), custom_call_target="tpu_custom_call" | custom-call | tf_op jit(solution)/shard_map/dispatch/pallas_call | solution.py:483
  75.8 0.0 copy-done
  75.8 78.8 %exchange.2.rows_ref = bf16[3,4,4,4,8,2048]{5,4,3,2,1,0:T(8,128)(2,1)} custom-call(bf16[3,4,4,4,8,2048]{5,4,3,2,1,0:T(8,128)(2,1)} %dispatch.1.src_ref), custom_call_target="tpu_custom_call" | custom-call | tf_op jit(solution)/shard_map/exchange/pallas_call | solution.py:443
  154.7 17.6 %experts.1.src_ref = bf16[3,4,4,4,8,2048]{5,4,3,2,1,0:T(8,128)(2,1)} custom-call(bf16[3,4,4,4,8,2048]{5,4,3,2,1,0:T(8,128)(2,1)} %exchange.2.rows_ref, bf16[2048,512]{1,0:T(8,128)(2,1)} %bitcast.8, bf16[2048,512]{1,0:T(8,128)(2,1)} %bitcast.9, bf16[512,2048]{1,0:T(8,128)(2,1)} %bitcast.10), custom_call_target="tpu_custom_call" | custom-call | tf_op jit(solution)/shard_map/experts/pallas_call | solution.py:506
  172.3 0.0 copy-start.3
  172.3 74.2 %exchange.3.back_ref = bf16[3,4,4,4,8,2048]{5,4,3,2,1,0:T(8,128)(2,1)} custom-call(bf16[3,4,4,4,8,2048]{5,4,3,2,1,0:T(8,128)(2,1)} %experts.1.src_ref), custom_call_target="tpu_custom_call" | custom-call | tf_op jit(solution)/shard_map/exchange/pallas_call | solution.py:443
  246.5 0.5 multiply_add_fusion.1.expert_ref
  247.0 0.0 copy-done.3
  247.1 0.1 copy.32
  247.2 5.8 %all_gather.7.weight_ref = f32[512,4]{1,0:T(8,128)} all-gather(f32[256,4]{1,0:T(8,128)S(1)} %copy.32), channel_id=1, replica_groups=mesh['sp_0'=4,'sp_1'=4,'sp_2'=4,'tp'=2] {'tp'}, dimensions={0}, use_global_device_ids=true | all-gather | bytes 12288 | tf_op jit(solution)/shard_map/all_gather | solution.py:618
  253.0 16.2 %combine.1 = bf16[256,2048]{1,0:T(8,128)(2,1)} custom-call(bf16[3,4,4,4,8,2048]{5,4,3,2,1,0:T(8,128)(2,1)} %exchange.3.back_ref, s32[512,4]{1,0:T(8,128)} %copy-done, s32[1,64]{1,0:T(1,128)} %multiply_add_fusion.1.expert_ref, f32[512,4]{1,0:T(8,128)} %all_gather.7.weight_ref, bf16[512,2048]{1,0:T(8,128)(2,1)} %get-tuple-element.13.normed_ref, ...), custom_call_target="tpu_custom_call" | custom-call | tf_op jit(solution)/shard_map/combine/pallas_call | solution.py:574
  269.1 2.3 copy.34
Async XLA Ops:
  1.4 2.5 copy-start.1
  24.0 39.5 %copy-start.2 = (s32[256,4]{0,1:T(4,128)S(1)}, s32[256,4]{0,1:T(4,128)}, u32[]{:S(2)}) copy-start(s32[256,4]{0,1:T(4,128)} %param.32) | copy-start | bytes 12292
  65.7 10.2 %copy-start = (s32[512,4]{1,0:T(8,128)}, s32[512,4]{1,0:T(8,128)S(1)}, u32[]{:S(2)}) copy-start(s32[512,4]{1,0:T(8,128)S(1)} %all_gather.6.ids_ref) | copy-start | bytes 24580
  172.3 74.7 %copy-start.3 = (f32[256,4]{0,1:T(4,128)S(1)}, f32[256,4]{0,1:T(4,128)}, u32[]{:S(2)}) copy-start(f32[256,4]{0,1:T(4,128)} %param.33) | copy-start | bytes 12292

commit v2 on v1

--- a/solution.py
+++ b/solution.py
@@ -237,8 +237,8 @@
 
 
 def mixed_kernel(
-    map_ref, z_ref, h_ref, gate_ref, gain_ref, out_w_ref, residual_ref, norm_ref,
-    attended_ref, normed_ref,
+    map_ref, z_ref, h_ref, gate_ref, gain_ref, out_w_ref, residual_ref, norm_ref, meta_ref,
+    attended_ref, normed_ref, both_meta_ref,
     row_s, plane_s, all_s, row_total, plane_total, state_out, state_in, mix_s, mix_in, acc_s,
     send_sem, recv_sem,
 ):
@@ -278,6 +278,16 @@
 
     sent = []
     copies = send(0, 2, lambda t: map_ref.at[t], row_s)
+    tell = pltpu.make_async_remote_copy(
+        src_ref=meta_ref,
+        dst_ref=both_meta_ref.at[c],
+        send_sem=send_sem.at[4, 2],
+        recv_sem=recv_sem.at[4, 2],
+        device_id=partner(),
+        device_id_type=MESH,
+    )
+    tell.start()
+    both_meta_ref[c] = meta_ref[...]
     row_s[x] = map_ref[x]
     for copy in copies:
         copy.wait_recv()
@@ -359,21 +369,23 @@
         device_id_type=MESH,
     )
     share.start()
+    tell.wait()
     share.wait()
     for copy in sent:
         copy.wait_send()
 
 
-def mixed(maps, z, h, gate, gain, out_w, residual, norm_gain):
+def mixed(maps, z, h, gate, gain, out_w, residual, norm_gain, meta):
     half, model = residual.shape
     return pl.pallas_call(
         mixed_kernel,
         out_shape=(
             jax.ShapeDtypeStruct((half, model), BF16),
             jax.ShapeDtypeStruct((2 * half, model), BF16),
+            jax.ShapeDtypeStruct((2,) + meta.shape, F32),
         ),
-        in_specs=[VMEM] * 8,
-        out_specs=(VMEM,) * 2,
+        in_specs=[VMEM] * 9,
+        out_specs=(VMEM,) * 3,
         scratch_shapes=[
             pltpu.VMEM((4, HD, 2 * HD), STATE_TYPE),
             pltpu.VMEM((4, HD, 2 * HD), STATE_TYPE),
@@ -390,80 +402,131 @@
         ],
         compiler_params=params(collective_id=0, has_side_effects=True),
         name="mixed",
-    )(maps, z, h, gate, gain, out_w, residual, norm_gain)
-
-
-def piece(ref, dim, i):
-    if dim == 0:
-        return ref.at[i]
-    if dim == 1:
-        return ref.at[:, i]
-    return ref.at[:, :, i]
-
-
-def exchange_kernel(src_ref, dst_ref, one_ref, two_ref, send_sem, recv_sem):
-    greet((0, 1, 2), False)
-    buffers = (src_ref, one_ref, two_ref, dst_ref)
-    sent = []
-    for stage in range(3):
-        copies = []
-        for n, off in enumerate(OFFSETS):
-            for k in range(3):
-                dim = ORDERS[k][stage]
-                here = lax.axis_index(AXES[dim])
-                copy = pltpu.make_async_remote_copy(
-                    src_ref=piece(buffers[stage].at[k], dim, lax.rem(here + off, 4)),
-                    dst_ref=piece(buffers[stage + 1].at[k], dim, here),
-                    send_sem=send_sem.at[stage, k, n],
-                    recv_sem=recv_sem.at[stage, k, n],
-                    device_id=along(dim, off),
-                    device_id_type=MESH,
-                )
-                copy.start()
-                copies.append(copy)
-        for k in range(3):
-            dim = ORDERS[k][stage]
-            here = lax.axis_index(AXES[dim])
-            source = piece(buffers[stage].at[k], dim, here)
-            target = piece(buffers[stage + 1].at[k], dim, here)
-
-            def keep(i, _):
-                target[i // 4, i % 4] = source[i // 4, i % 4]
-                return 0
-
-            lax.fori_loop(0, 16, keep, 0)
-        for copy in copies:
-            copy.wait_recv()
-        sent += copies
-    for copy in sent:
-        copy.wait_send()
-
-
-def exchange(rows):
-    return pl.pallas_call(
-        exchange_kernel,
-        out_shape=jax.ShapeDtypeStruct(rows.shape, rows.dtype),
-        in_specs=[VMEM],
-        out_specs=VMEM,
-        scratch_shapes=[pltpu.VMEM(rows.shape, rows.dtype)] * 2
-        + [pltpu.SemaphoreType.DMA((3, 3, 3))] * 2,
-        compiler_params=params(collective_id=1, has_side_effects=True),
-        name="exchange",
-    )(rows)
-
-
-def dispatch_kernel(normed_ref, ids_ref, expert_ref, rows_ref, code_s):
-    tokens = normed_ref.shape[0]
+    )(maps, z, h, gate, gain, out_w, residual, norm_gain, meta)
+
+
+def at(ref, fixed):
+    return ref.at[tuple(fixed.get(d, slice(None)) for d in range(3))]
+
+
+def experts_kernel(
+    normed_ref, attended_ref, meta_ref, gate_hbm, up_hbm, down_hbm, common_gate_hbm, common_up_hbm, common_down_hbm,
+    out_ref,
+    buf0, buf1, buf2, buf3, buf4, gate_w, up_w, down_w, common_gate_w, common_up_w, common_down_w,
+    code_s, pick_s, acc_s, away_s, here_s,
+    send1, recv1, send2, recv2, send3, recv3, free_sem, swap_send, swap_recv, load_sem,
+):
+    tokens, model = normed_ref.shape
     half = tokens // 2
-    chips = expert_ref.shape[0]
+    chips = 64
+    c = lax.axis_index("tp")
+    loads = [
+        pltpu.make_async_copy(a, b, load_sem.at[i])
+        for i, (a, b) in enumerate(
+            (
+                (common_gate_hbm, common_gate_w),
+                (common_up_hbm, common_up_w),
+                (common_down_hbm, common_down_w),
+                (gate_hbm, gate_w),
+                (up_hbm, up_w),
+                (down_hbm, down_w),
+            )
+        )
+    ]
+    for load in loads:
+        load.start()
+
+    coord = [lax.axis_index(a) for a in SP]
+    away = [[lax.rem(coord[d] + off, 4) for off in OFFSETS] for d in range(3)]
+    back = [[lax.rem(coord[d] + 4 - off, 4) for off in OFFSETS] for d in range(3)]
+    forward = (buf0, buf1, buf2, buf3)
+    backward = (buf3, buf4, buf1, buf0)
+
+    def dims(way, k):
+        return ORDERS[k] if way == 0 else ORDERS[k][::-1]
+
+    def remote(src, dst, send, recv, dim, n):
+        return pltpu.make_async_remote_copy(
+            src_ref=src,
+            dst_ref=dst,
+            send_sem=send,
+            recv_sem=recv,
+            device_id=along(dim, OFFSETS[n]),
+            device_id_type=MESH,
+        )
+
+    def keep(source, target):
+        for i in range(4):
+            target[i] = source[i]
+
+    def first(way, k, n):
+        bufs = forward if way == 0 else backward
+        d1 = dims(way, k)[0]
+        return remote(
+            at(bufs[0].at[k], {d1: away[d1][n]}),
+            at(bufs[1].at[k], {d1: coord[d1]}),
+            send1.at[way, k, n],
+            recv1.at[way, k, n],
+            d1,
+            n,
+        )
+
+    def second(way, k, m, n):
+        bufs = forward if way == 0 else backward
+        d1, d2, _ = dims(way, k)
+        source = bufs[0] if m == 0 else bufs[1]
+        place = coord[d1] if m == 0 else back[d1][m - 1]
+        return remote(
+            at(source.at[k], {d1: place, d2: away[d2][n]}),
+            at(bufs[2].at[k], {d1: place, d2: coord[d2]}),
+            send2.at[way, k, m, n],
+            recv2.at[way, k, m, n],
+            d2,
+            n,
+        )
+
+    def third(way, k, m, n):
+        bufs = forward if way == 0 else backward
+        _, d2, d3 = dims(way, k)
+        place = coord[d2] if m == 0 else back[d2][m - 1]
+        return remote(
+            at(bufs[2].at[k], {d2: place, d3: away[d3][n]}),
+            at(bufs[3].at[k], {d2: place, d3: coord[d3]}),
+            send3.at[way, k, m, n],
+            recv3.at[way, k, m, n],
+            d3,
+            n,
+        )
+
+    def start_second(way, k, m):
+        bufs = forward if way == 0 else backward
+        d1, d2, _ = dims(way, k)
+        for n in range(3):
+            second(way, k, m, n).start()
+        source = bufs[0] if m == 0 else bufs[1]
+        place = coord[d1] if m == 0 else back[d1][m - 1]
+        keep(at(source.at[k], {d1: place, d2: coord[d2]}), at(bufs[2].at[k], {d1: place, d2: coord[d2]}))
+
+    def start_third(way, k, m):
+        bufs = forward if way == 0 else backward
+        _, d2, d3 = dims(way, k)
+        for n in range(3):
+            third(way, k, m, n).start()
+        place = coord[d2] if m == 0 else back[d2][m - 1]
+        keep(at(bufs[2].at[k], {d2: place, d3: coord[d3]}), at(bufs[3].at[k], {d2: place, d3: coord[d3]}))
+
+    expert = (2 * iota((chips, 1), 0) + c).astype(F32)
     chosen = jnp.zeros((chips, tokens), F32)
     for j in range(TOP_K):
-        chosen = chosen + jnp.where(ids_ref[j : j + 1, :] == expert_ref[...], 1.0, 0.0)
+        ids = jnp.concatenate([meta_ref[0, j : j + 1, :], meta_ref[1, j : j + 1, :]], 1)
+        chosen = chosen + jnp.where(ids == expert, 1.0, 0.0)
     i, j = iota((tokens, tokens), 0), iota((tokens, tokens), 1)
-    before = jnp.where((i // half == j // half) & (i < j), 1.0, 0.0).astype(BF16)
+    same = i // half == j // half
+    before = jnp.where(same & (i < j), 1.0, 0.0).astype(BF16)
     slot = mm(chosen.astype(BF16), before)
     shift = jnp.where(iota((chips, tokens), 1) < half, 0.0, float(CAP))
     code_s[...] = jnp.where(chosen > 0.0, slot + shift, -1.0)
+    greet((0, 1, 2), True)
     for k in range(3):
         low = 0 if k < 2 else half
         high = half if k == 0 else tokens
@@ -473,63 +536,40 @@
             wanted = (iota((16, 8, high - low), 1) + 8 * k).astype(F32)
             pick = jnp.where(code[:, None, :] == wanted, 1.0, 0.0).reshape(128, high - low).astype(BF16)
             rows = mm(pick, normed_ref[low:high, :]).astype(BF16)
-            rows_ref[k, zi] = rows.reshape(4, 4, 8, rows.shape[-1])
+            buf0[k, zi] = rows.reshape(4, 4, 8, model)
             return 0
 
         lax.fori_loop(0, 4, one, 0)
-
-
-def dispatch(normed, ids, experts):
-    return pl.pallas_call(
-        dispatch_kernel,
-        out_shape=jax.ShapeDtypeStruct((3, 4, 4, 4, 8, normed.shape[1]), BF16),
-        in_specs=[VMEM] * 3,
-        out_specs=VMEM,
-        scratch_shapes=[pltpu.VMEM((64, normed.shape[0]), F32)],
-        compiler_params=params(),
-        name="dispatch",
-    )(normed, ids, experts)
-
-
-def experts_kernel(rows_ref, gate_ref, up_ref, down_ref, out_ref):
-    def one(k, _):
-        rows = rows_ref[k].reshape(512, rows_ref.shape[-1])
-        hidden = silu(mm(rows, gate_ref[...])) * mm(rows, up_ref[...])
-        result = mm(hidden.astype(BF16), down_ref[...]).astype(BF16)
-        out_ref[k] = result.reshape(out_ref.shape[1:])
-        return 0
-
-    lax.fori_loop(0, 3, one, 0)
-
-
-def run_experts(rows, gate, up, down):
-    return pl.pallas_call(
-        experts_kernel,
-        out_shape=jax.ShapeDtypeStruct(rows.shape, BF16),
-        in_specs=[VMEM] * 4,
-        out_specs=VMEM,
-        compiler_params=params(),
-        name="experts",
-    )(rows, gate, up, down)
-
-
-def combine_kernel(
-    back_ref, ids_ref, expert_ref, weight_ref, normed_ref, attended_ref, gate_ref, up_ref, down_ref,
-    out_ref, pick_s, away_s, here_s, send_sem, recv_sem,
-):
-    greet((), True)
-    tokens, model = normed_ref.shape
-    half = tokens // 2
-    chips = expert_ref.shape[1]
-    c = lax.axis_index("tp")
+        for n in range(3):
+            first(0, k, n).start()
+    for k in range(3):
+        start_second(0, k, 0)
+
+    for load in loads[:3]:
+        load.wait()
+    own = pl.ds(pl.multiple_of(c * half, half), half)
+    hidden = silu(mm(normed_ref[own, :], common_gate_w[...])) * mm(normed_ref[own, :], common_up_w[...])
+    hidden = hidden.astype(BF16)
+    for n in range(model // 512):
+        cols = slice(512 * n, 512 * n + 512)
+        acc_s[:, cols] = attended_ref[:, cols].astype(F32) + mm(hidden, common_down_w[:, cols])
+
+    for n in range(3):
+        for k in range(3):
+            first(0, k, n).wait_recv()
+            start_second(0, k, n + 1)
+    for k in range(3):
+        start_third(0, k, 0)
+
+    meta = jnp.concatenate([meta_ref[0], meta_ref[1]], 1).T
+    expert = (2 * iota((1, chips), 1) + c).astype(F32)
     chosen = jnp.zeros((tokens, chips), F32)
     weight = jnp.zeros((tokens, chips), F32)
-    for j in range(TOP_K):
-        hit = ids_ref[:, j : j + 1] == expert_ref[...]
+    for q in range(TOP_K):
+        hit = meta[:, q : q + 1] == expert
         chosen = chosen + jnp.where(hit, 1.0, 0.0)
-        weight = weight + jnp.where(hit, weight_ref[:, j : j + 1], 0.0)
-    i, j = iota((tokens, tokens), 0), iota((tokens, tokens), 1)
-    before = jnp.where((i // half == j // half) & (j < i), 1.0, 0.0).astype(BF16)
+        weight = weight + jnp.where(hit, meta[:, TOP_K + q : TOP_K + q + 1], 0.0)
+    before = jnp.where(same & (j < i), 1.0, 0.0).astype(BF16)
     slot = mm(before, chosen.astype(BF16))
     shift = jnp.where(iota((tokens, chips), 0) < half, 0.0, float(CAP))
     code = jnp.where(chosen > 0.0, slot + shift, -1.0).astype(BF16)
@@ -540,52 +580,129 @@
     for k in range(3):
         pick_s[k] = jnp.where(code == place + 8.0 * k, weight, 0.0).astype(BF16)
 
-    def partial(core, n):
+    for n in range(3):
+        for k in range(3):
+            for m in range(4):
+                second(0, k, m, n).wait_recv()
+            start_third(0, k, n + 1)
+    for k in range(3):
+        for n in range(3):
+            first(0, k, n).wait_send()
+        for m in range(4):
+            for n in range(3):
+                second(0, k, m, n).wait_send()
+        d1, d2, _ = ORDERS[k]
+        for off in OFFSETS:
+            pl.semaphore_signal(free_sem.at[0, k], inc=1, device_id=along(d2, off), device_id_type=MESH)
+            pl.semaphore_signal(free_sem.at[1, k], inc=1, device_id=along(d1, off), device_id_type=MESH)
+    for load in loads[3:]:
+        load.wait()
+
+    def serve(places):
+        views = [at(buf3.at[k], {ORDERS[k][2]: places[k]}) for k in range(3)]
+        rows = jnp.concatenate([v[...].reshape(128, model) for v in views], 0)
+        hidden = (silu(mm(rows, gate_w[...])) * mm(rows, up_w[...])).astype(BF16)
+        for n in range(model // 512):
+            cols = slice(512 * n, 512 * n + 512)
+            result = mm(hidden, down_w[:, cols]).astype(BF16)
+            for k in range(3):
+                views[k][:, :, :, cols] = result[128 * k : 128 * k + 128].reshape(4, 4, 8, 512)
+
+    last = [ORDERS[k][2] for k in range(3)]
+    serve([coord[d] for d in last])
+    for k in range(3):
+        pl.semaphore_wait(free_sem.at[0, k], 3)
+        start_second(1, k, 0)
+    for n in range(3):
+        for k in range(3):
+            for m in range(4):
+                third(0, k, m, n).wait_recv()
+        serve([back[d][n] for d in last])
+        turned = OFFSETS.index(4 - OFFSETS[n])
+        for k in range(3):
+            first(1, k, turned).start()
+    for n in range(3):
+        for k in range(3):
+            first(1, k, n).wait_recv()
+            start_second(1, k, n + 1)
+    for k in range(3):
+        pl.semaphore_wait(free_sem.at[1, k], 3)
+        start_third(1, k, 0)
+    for n in range(3):
+        for k in range(3):
+            for m in range(4):
+                second(1, k, m, n).wait_recv()
+            start_third(1, k, n + 1)
+    for n in range(3):
+        for k in range(3):
+            for m in range(4):
+                third(1, k, m, n).wait_recv()
+
+    def partial(core, cols):
         rows = pl.ds(pl.multiple_of(core * half, half), half)
-        cols = slice(512 * n, 512 * n + 512)
-        total = jnp.zeros((half, 512), F32)
-        for k in range(3):
-            total = total + mm(pick_s[k, rows, :], back_ref[k, :, :, :, :, cols].reshape(8 * chips, 512))
-        return total
-
+        total = mm(pick_s[1, rows, :], buf0[1, :, :, :, :, cols].reshape(8 * chips, 512))
+        return total + mm(pick_s[2 * core, rows, :], buf0[2 * core, :, :, :, :, cols].reshape(8 * chips, 512))
+
+    swaps = []
     for n in range(model // 512):
-        away_s[:, 512 * n : 512 * n + 512] = partial(1 - c, n)
-    copy = pltpu.make_async_remote_copy(
-        src_ref=away_s,
-        dst_ref=here_s,
-        send_sem=send_sem,
-        recv_sem=recv_sem,
-        device_id=partner(),
-        device_id_type=MESH,
-    )
-    copy.start()
-    own = pl.ds(pl.multiple_of(c * half, half), half)
-    rows = normed_ref[own, :]
-    hidden = (silu(mm(rows, gate_ref[...])) * mm(rows, up_ref[...])).astype(BF16)
-    copy.wait()
+        away_s[n] = partial(1 - c, slice(512 * n, 512 * n + 512))
+        swap = pltpu.make_async_remote_copy(
+            src_ref=away_s.at[n],
+            dst_ref=here_s.at[n],
+            send_sem=swap_send.at[n],
+            recv_sem=swap_recv.at[n],
+            device_id=partner(),
+            device_id_type=MESH,
+        )
+        swap.start()
+        swaps.append(swap)
     for n in range(model // 512):
         cols = slice(512 * n, 512 * n + 512)
-        total = attended_ref[:, cols].astype(F32) + mm(hidden, down_ref[:, cols])
-        out_ref[:, cols] = (total + (partial(c, n) + here_s[:, cols])).astype(BF16)
-
-
-def combine(back, ids, experts, weight, normed, attended, gate, up, down):
+        acc_s[:, cols] = acc_s[:, cols] + partial(c, cols)
+    for n in range(model // 512):
+        cols = slice(512 * n, 512 * n + 512)
+        swaps[n].wait()
+        out_ref[:, cols] = (acc_s[:, cols] + here_s[n]).astype(BF16)
+
+    for k in range(3):
+        for m in range(4):
+            for n in range(3):
+                third(0, k, m, n).wait_send()
+                second(1, k, m, n).wait_send()
+                third(1, k, m, n).wait_send()
+        for n in range(3):
+            first(1, k, n).wait_send()
+
+
+def run_experts(normed, attended, meta, gate, up, down, common_gate, common_up, common_down):
     half, model = attended.shape
+    buffer = pltpu.VMEM((3, 4, 4, 4, 8, model), BF16)
+    hbm = pl.BlockSpec(memory_space=pl.ANY)
     return pl.pallas_call(
-        combine_kernel,
+        experts_kernel,
         out_shape=jax.ShapeDtypeStruct((half, model), BF16),
-        in_specs=[VMEM] * 9,
+        in_specs=[VMEM] * 3 + [hbm] * 6,
         out_specs=VMEM,
-        scratch_shapes=[
+        scratch_shapes=[buffer] * 5
+        + [pltpu.VMEM(w.shape, BF16) for w in (gate, up, down, common_gate, common_up, common_down)]
+        + [
+            pltpu.VMEM((64, 2 * half), F32),
             pltpu.VMEM((3, 2 * half, 512), BF16),
             pltpu.VMEM((half, model), F32),
-            pltpu.VMEM((half, model), F32),
-            pltpu.SemaphoreType.DMA,
-            pltpu.SemaphoreType.DMA,
+            pltpu.VMEM((model // 512, half, 512), F32),
+            pltpu.VMEM((model // 512, half, 512), F32),
+        ]
+        + [pltpu.SemaphoreType.DMA((2, 3, 3))] * 2
+        + [pltpu.SemaphoreType.DMA((2, 3, 4, 3))] * 4
+        + [
+            pltpu.SemaphoreType.REGULAR((2, 3)),
+            pltpu.SemaphoreType.DMA((model // 512,)),
+            pltpu.SemaphoreType.DMA((model // 512,)),
+            pltpu.SemaphoreType.DMA((6,)),
         ],
-        compiler_params=params(collective_id=2, has_side_effects=True),
-        name="combine",
-    )(back, ids, experts, weight, normed, attended, gate, up, down)
+        compiler_params=params(collective_id=1, has_side_effects=True),
+        name="experts",
+    )(normed, attended, meta, gate, up, down, common_gate, common_up, common_down)
 
 
 def shards(
@@ -614,11 +731,9 @@
     decay = extra_log_decay - jnp.exp(head_rate_logarithm)[None, :] * jax.nn.softplus(
         decay_input_logits.astype(F32) - 6.0
     )
-    ids = lax.all_gather(selected_expert_index, "tp", tiled=True)
-    weight = lax.all_gather(routing_weight, "tp", tiled=True)
-    experts = 2 * jnp.arange(64, dtype=jnp.int32) + lax.axis_index("tp").astype(jnp.int32)
+    meta = jnp.concatenate([selected_expert_index.T.astype(F32), routing_weight.T], 0)
     maps, z, h = local_terms(projected_queries, projected_keys, projected_values, beta, decay)
-    attended, normed = mixed(
+    attended, normed, meta = mixed(
         maps,
         z,
         h,
@@ -627,18 +742,15 @@
         output_matrix,
         residual,
         mixture_norm_gain[None, :],
+        meta,
     )
-    outgoing = dispatch(normed, ids.T, experts[:, None])
-    arrived = exchange(outgoing)
-    served = run_experts(arrived, routed_gate_weight[0], routed_up_weight[0], routed_down_weight[0])
-    back = exchange(served)
-    return combine(
-        back,
-        ids,
-        experts[None, :],
-        weight,
+    return run_experts(
         normed,
         attended,
+        meta,
+        routed_gate_weight[0],
+        routed_up_weight[0],
+        routed_down_weight[0],
         common_gate_weight,
         common_up_weight,
         common_down_weight,

time: 272 us -> 223 us (0.82)
  Pallas kernels: 255 us -> 215 us
  blocking collectives: 7.76 us -> 0 us
    pallas_call x5 -> x1, Pallas kernels: 196 us -> 155 us  [run_experts(): pl.pallas_call(experts_kernel, out_shape=jax.ShapeDtypeStruct((half, mode...]
    all_gather x2 -> x0, blocking collectives: 7.76 us -> none  [the longest x1 5.76 us: shards(): weight = lax.all_gather(routing_weight, 'tp', tiled=True)]
where the time goes in v2:
time: 223 us
  Pallas kernels  215 us (96%)
  local copies, waits for them, and re-layouts  4.68 us (2%)
  other arithmetic  3.52 us (2%)
    pallas_call x1, Pallas kernels, run_experts(): pl.pallas_call(experts_kernel, out_shape=jax.ShapeDtypeStruct((half, mode...  155 us
    pallas_call x1, Pallas kernels, mixed(): pl.pallas_call(mixed_kernel, out_shape=(jax.ShapeDtypeStruct((half, model...  39.5 us
    pallas_call x1, Pallas kernels, local_terms(): pl.pallas_call(local_kernel, out_shape=(jax.ShapeDtypeStruct((heads, HD,...  20.1 us

profile of v2, /device:TPU:1, one launch (start us, length us, event | category | flops | bytes accessed | tf_op | source)
XLA Modules:
  0.0 222.7 jit_solution(6740935044820642647)
XLA Ops:
  0.0 0.7 exp.11
  0.7 0.7 convert_bitcast_fusion
  1.4 1.3 pad_maximum_fusion.meta_ref
  2.6 0.8 fusion.1
  3.4 0.0 copy-start
  3.4 0.9 copy.26.decay_ref
  4.3 0.8 copy.23
  5.1 0.8 add_divide_fusion.beta_ref
  5.9 0.0 copy-done
  5.9 20.1 %local_terms.1 = (bf16[4,128,256]{2,1,0:T(8,128)(2,1)}, f32[4,512,128]{2,1,0:T(8,128)}, f32[4,512,128]{2,1,0:T(8,128)}) custom-call(bf16[512,512]{1,0:T(8,128)(2,1)} %q_ref.1, bf16[512,512]{1,0:T(8,128)(2,1)} %k_ref.1, bf16[512,512]{1,0:T(8,128)(2,1)} %v_ref.1, f32[512,4]{1,0:T(8,128)} %add_divide_fusion.beta_ref, f32[512,4]{1,0:T(8,128)} %copy.26.decay_ref, ...), custom_call_target="tpu_custom_call" | custom-call | tf_op jit(solution)/shard_map/local_terms/pallas_call | solution.py:188
  26.0 39.5 %mixed.1 = (bf16[256,2048]{1,0:T(8,128)(2,1)}, bf16[512,2048]{1,0:T(8,128)(2,1)}, f32[2,8,256]{2,1,0:T(8,128)}) custom-call(bf16[4,128,256]{2,1,0:T(8,128)(2,1)} %get-tuple-element.11.map_ref, f32[4,512,128]{2,1,0:T(8,128)} %get-tuple-element.12.z_ref, f32[4,512,128]{2,1,0:T(8,128)} %get-tuple-element.13.h_ref, bf16[512,512]{1,0:T(8,128)(2,1)} %gate_ref.1, ...), custom_call_target="tpu_custom_call" | custom-call | tf_op jit(solution)/shard_map/mixed/pallas_call | solution.py:380
  65.5 154.9 %experts.1 = bf16[256,2048]{1,0:T(8,128)(2,1)} custom-call(bf16[512,2048]{1,0:T(8,128)(2,1)} %get-tuple-element.14.normed_ref, bf16[256,2048]{1,0:T(8,128)(2,1)} %get-tuple-element.15.attended_ref, f32[2,8,256]{2,1,0:T(8,128)} %get-tuple-element.16.meta_ref, bf16[2048,512]{1,0:T(8,128)(2,1)} %bitcast.9, bf16[2048,512]{1,0:T(8,128)(2,1)} %bitcast.10, ...), custom_call_target="tpu_custom_call" | custom-call | tf_op jit(solution)/shard_map/experts/pallas_call | solution.py:681
  220.4 2.3 %copy.28 = bf16[256,2048]{1,0:T(8,128)(2,1)} copy(bf16[256,2048]{1,0:T(8,128)(2,1)} %experts.1) | data formatting | bytes 2097152
Async XLA Ops:
  3.4 2.5 %copy-start = (f32[512,4]{0,1:T(4,128)}, f32[512,4]{0,1:T(4,128)S(1)}, u32[]{:S(2)}) copy-start(f32[512,4]{0,1:T(4,128)S(1)} %fusion.1) | copy-start | bytes 24580

commit v3 on v2

--- a/solution.py
+++ b/solution.py
@@ -38,8 +38,15 @@
 
 
 def mm3(a, b, dims=((1,), (0,))):
-    (ah, al), (bh, bl) = a, b
-    return mm(ah, bh, dims) + mm(al, bh, dims) + mm(ah, bl, dims)
+    high, low = a
+    both = mm2(a, b[0], dims)
+    return both + mm(high, b[1], dims)
+
+
+def mm2(a, b, dims=((1,), (0,))):
+    rows = a[0].shape[0]
+    both = mm(jnp.concatenate(a, 0), b, dims)
+    return both[:rows] + both[rows:]
 
 
 def silu(x):
@@ -50,29 +57,80 @@
     return lax.broadcasted_iota(jnp.int32, shape, dim)
 
 
-def local_kernel(
-    q_ref, k_ref, v_ref, beta_ref, decay_ref, decay_t_ref,
-    map_ref, z_ref, h_ref,
-    low_s, score_s, inv_s, right_s, qd_s, kdt_s, wu_s, qp_s, step_s, pre_s,
+def along(dim, off):
+    at = [lax.axis_index(a) for a in AXES]
+    at[dim] = lax.rem(at[dim] + off, 4)
+    return tuple(at)
+
+
+def partner():
+    at = [lax.axis_index(a) for a in AXES]
+    at[3] = 1 - at[3]
+    return tuple(at)
+
+
+def greet(dims, pair):
+    pl.semaphore_wait(pltpu.get_barrier_semaphore(), arrive(dims, pair))
+
+
+def arrive(dims, pair):
+    barrier = pltpu.get_barrier_semaphore()
+    count = 0
+    for dim in dims:
+        for off in OFFSETS:
+            pl.semaphore_signal(barrier, inc=1, device_id=along(dim, off), device_id_type=MESH)
+            count += 1
+    if pair:
+        pl.semaphore_signal(barrier, inc=1, device_id=partner(), device_id_type=MESH)
+        count += 1
+    return count
+
+
+def attention_kernel(
+    q_ref, k_ref, v_ref, strength_ref, input_ref, extra_ref, rate_ref, gate_hbm, gain_ref, out_w_hbm, residual_hbm,
+    norm_ref, ids_ref, weight_ref,
+    attended_ref, normed_ref, both_meta_ref,
+    beta_s, g_s, row_s, low_s, score_s, inv_s, right_s, qd_s, kdt_s, qp_s, step_s, pre_s, z_s, h_s, map_s, meta_s,
+    gate_s, out_w_s, residual_s, lit_s, rows_in, plane_in, all_in, row_total, plane_total, state_out, state_in,
+    mix_s, mix_in, acc_s, send_sem, recv_sem, load_sem,
 ):
     heads, tokens = 4, q_ref.shape[0]
     blocks = tokens // SPAN
+    loads = [
+        pltpu.make_async_copy(src, dst, load_sem.at[i])
+        for i, (src, dst) in enumerate(((gate_hbm, gate_s), (residual_hbm, residual_s), (out_w_hbm, out_w_s)))
+    ]
+    for load in loads:
+        load.start()
+    greeted = arrive((0, 1, 2), True)
+    z, y, x, c = (lax.axis_index(a) for a in AXES)
+    meta_s[0:TOP_K, :] = ids_ref[...].astype(F32)
+    meta_s[TOP_K : 2 * TOP_K, :] = weight_ref[...]
+
     i256, j256 = iota((256, 256), 0), iota((256, 256), 1)
     same = (i256 // SPAN) == (j256 // SPAN)
-    tri = jnp.where(same & (j256 <= i256), 1.0, 0.0)
     tri_t = jnp.where(same & (i256 <= j256), 1.0, 0.0)
     ones = jnp.where(same, 1.0, 0.0)
 
     def high(a, b):
         return lax.dot_general(a, b, (((1,), (0,)), ((), ())), precision=HIGH, preferred_element_type=F32)
 
-    dec = [decay_ref[256 * i : 256 * i + 256, :] for i in range(2)]
-    dec_t = [decay_t_ref[:, 256 * i : 256 * i + 256] for i in range(2)]
-    g_col = jnp.concatenate([high(tri, d) for d in dec], 0)
-    total_col = jnp.concatenate([high(ones, d) for d in dec], 0)
-    g_row = jnp.concatenate([high(d, tri_t) for d in dec_t], 1)
-    total_row = jnp.concatenate([high(d, ones) for d in dec_t], 1)
-    beta = beta_ref[...]
+    rate = jnp.where(iota((heads, heads), 0) == iota((heads, heads), 1), jnp.exp(rate_ref[...]), 0.0)
+    rate = jnp.sum(rate, axis=1, keepdims=True)
+    grown = input_ref[...].astype(F32) - 6.0
+    tail = jnp.exp(-jnp.abs(grown))
+    up = 1.0 + tail
+    log_up = jnp.where(up == 1.0, tail, jnp.log(up) * tail / jnp.where(up == 1.0, 1.0, up - 1.0))
+    decay = extra_ref[...] - rate * (jnp.maximum(grown, 0.0) + log_up)
+    beta = 1.0 / (1.0 + jnp.exp(-strength_ref[...].astype(F32)))
+    g_row = jnp.concatenate([high(decay[:, 256 * i : 256 * i + 256], tri_t) for i in range(2)], 1)
+    total_row = jnp.concatenate([high(decay[:, 256 * i : 256 * i + 256], ones) for i in range(2)], 1)
+    row_s[0:heads, :] = g_row
+    row_s[heads : 2 * heads, :] = total_row
+    cols = jnp.concatenate([beta, g_row], 0).T
+    for h in range(heads):
+        beta_s[h] = jnp.broadcast_to(cols[:, h : h + 1], (tokens, HD))
+        g_s[h] = jnp.broadcast_to(cols[:, heads + h : heads + h + 1], (tokens, HD))
 
     row, lane = iota((SPAN, 128), 0), iota((SPAN, 128), 1)
     first = lane < SPAN
@@ -82,21 +140,21 @@
     first_wide = iota((128, 128), 1) < SPAN
     eye = jnp.where(iota((128, 128), 0) == iota((128, 128), 1), 1.0, 0.0)
 
-    for h in range(heads):
-        cols = slice(h * HD, h * HD + HD)
-        q = silu(q_ref[:, cols].astype(F32))
+    def prepare(h, _):
+        lanes = pl.ds(pl.multiple_of(h * HD, HD), HD)
+        q = silu(q_ref[:, lanes].astype(F32))
         q = q * lax.rsqrt(jnp.sum(q * q, axis=-1, keepdims=True) + EPS)
-        k = silu(k_ref[:, cols].astype(F32))
+        k = silu(k_ref[:, lanes].astype(F32))
         k = k * lax.rsqrt(jnp.sum(k * k, axis=-1, keepdims=True) + EPS)
-        v = silu(v_ref[:, cols].astype(F32))
-        b_h, g_h = beta[:, h : h + 1], g_col[:, h : h + 1]
+        v = silu(v_ref[:, lanes].astype(F32))
+        b_h, g_h = beta_s[h], g_s[h]
         grown = jnp.exp(g_h)
         kb = k * b_h
-        right_s[h, :, :HD] = kb * grown
-        right_s[h, :, HD:] = v * b_h
+        right_s[h, :, :HD] = (kb * grown).astype(BF16)
+        right_s[h, :, HD:] = (v * b_h).astype(BF16)
         qd_s[h] = q * grown
-        gr = g_row[h : h + 1, :]
-        kdt_s[h] = k.T * jnp.exp(total_row[h : h + 1, :] - gr)
+        gr = row_s[pl.ds(h, 1), :]
+        kdt_s[h] = k.T * jnp.exp(row_s[pl.ds(h + heads, 1), :] - gr)
         ks, kbs, qs = halves(k), halves(kb), halves(q)
         for j in range(tokens // 128):
             rows = slice(128 * j, 128 * j + 128)
@@ -109,6 +167,9 @@
             decay = jnp.where(causal, jnp.exp(spread), 0.0)
             low_s[h, :, rows] = jnp.where(strict, inner * decay, 0.0)
             score_s[h, :, rows] = score * decay
+        return 0
+
+    lax.fori_loop(0, heads, prepare, 0)
 
     r4, l4 = iota((SPAN, 256), 0), iota((SPAN, 256), 1)
     p4 = l4 % SPAN
@@ -121,9 +182,11 @@
     def times(a, b):
         return mm3(a, tuple(diag4(x) for x in b))
 
-    groups = [(h, slice(256 * i, 256 * i + 256)) for h in range(heads) for i in range(2)]
-    for part in range(2):
-        mine = groups[4 * part : 4 * part + 4]
+    def times2(a, b):
+        return mm2(a, diag4(b.astype(BF16)))
+
+    def invert(part, _):
+        mine = [(2 * part + i // 2, slice(256 * (i % 2), 256 * (i % 2) + 256)) for i in range(4)]
         lows = [low_s[h, :, s] for h, s in mine]
         small = r4 // 8 == p4 // 8
         d1 = [jnp.where(small, x, 0.0) for x in lows]
@@ -135,115 +198,52 @@
         inv = [x + times(halves(x), d) for x, d in zip(x2, d4s)]
         for size in (8, 16, 32):
             off = (r4 // (2 * size) == p4 // (2 * size)) & (r4 // size != p4 // size)
-            invs = [halves(x) for x in inv]
-            ex = [halves(times(halves(jnp.where(off, x, 0.0)), y)) for x, y in zip(lows, invs)]
-            inv = [x - times(y, e) for x, y, e in zip(inv, invs, ex)]
+            ex = [times2(halves(jnp.where(off, x, 0.0)), y) for x, y in zip(lows, inv)]
+            inv = [x - times2(halves(x), e) for x, e in zip(inv, ex)]
         for (h, s), x in zip(mine, inv):
             inv_s[h, :, s] = x
+        return 0
+
+    lax.fori_loop(0, 2, invert, 0)
 
     def diag2(x):
         return jnp.concatenate([x * m for m in pair_masks], 0)
 
-    for h in range(heads):
+    def apply(h, _):
         for j in range(tokens // 128):
             rows = slice(128 * j, 128 * j + 128)
             inv = tuple(diag2(x) for x in halves(inv_s[h, :, rows]))
-            wu = mm3(inv, halves(right_s[h, rows, :]))
-            wus = halves(wu)
-            score = tuple(diag2(x) for x in halves(score_s[h, :, rows]))
-            applied = mm3(score, wus)
-            qp_s[h, rows, :] = qd_s[h, rows, :] - applied[:, :HD]
-            h_ref[h, rows, :] = applied[:, HD:]
+            wu = mm2(inv, right_s[h, rows, :]).astype(BF16)
+            score = [diag2(x) for x in halves(score_s[h, :, rows])]
             kdt = kdt_s[h, :, rows]
-            kdt = jnp.concatenate([jnp.where(first_wide, kdt, 0.0), jnp.where(first_wide, 0.0, kdt)], 0)
-            change = mm3(halves(kdt), wus)
-            for c in range(2):
-                n = 2 * j + c
-                factor = jnp.exp(total_col[n * SPAN : n * SPAN + 1, h : h + 1])
-                step_s[h, n, :, :HD] = eye * factor - change[128 * c : 128 * c + 128, :HD]
-                step_s[h, n, :, HD:] = change[128 * c : 128 * c + 128, HD:]
+            kdt = halves(jnp.concatenate([jnp.where(first_wide, kdt, 0.0), jnp.where(first_wide, 0.0, kdt)], 0))
+            left = tuple(jnp.concatenate([a, b], 0) for a, b in zip(score, kdt))
+            both = mm2(left, wu)
+            qp_s[h, rows, :] = qd_s[h, rows, :] - both[:128, :HD]
+            h_s[h, rows, :] = both[:128, HD:]
+            change = both[128:]
+            for i in range(2):
+                n = 2 * j + i
+                factor = jnp.exp(g_s[h, n * SPAN + SPAN - 1 : n * SPAN + SPAN, :])
+                step_s[h, n, :, :HD] = eye * factor - change[128 * i : 128 * i + 128, :HD]
+                step_s[h, n, :, HD:] = change[128 * i : 128 * i + 128, HD:]
+        return 0
+
+    lax.fori_loop(0, heads, apply, 0)
 
     for h in range(heads):
-        pre_s[h, 1] = step_s[h, 0]
-    for n in range(1, blocks):
+        pre_s[1, h] = step_s[h, 0]
+
+    def grow(n, _):
         for h in range(heads):
-            moved = mm3(halves(step_s[h, n, :, :HD]), halves(pre_s[h, n]))
-            pre = jnp.concatenate([moved[:, :HD], moved[:, HD:] + step_s[h, n, :, HD:]], 1)
-            if n + 1 < blocks:
-                pre_s[h, n + 1] = pre
-            else:
-                map_ref[h] = pre.astype(map_ref.dtype)
+            moved = mm3(halves(step_s[h, n, :, :HD]), halves(pre_s[n, h]))
+            pre_s[n + 1, h, :, :HD] = moved[:, :HD]
+            pre_s[n + 1, h, :, HD:] = moved[:, HD:] + step_s[h, n, :, HD:]
+        return 0
+
+    lax.fori_loop(1, blocks, grow, 0)
     for h in range(heads):
-        z_ref[h, 0:SPAN, :] = qp_s[h, 0:SPAN, :]
-        for n in range(1, blocks):
-            rows = slice(SPAN * n, SPAN * n + SPAN)
-            moved = mm3(halves(qp_s[h, rows, :]), halves(pre_s[h, n]))
-            z_ref[h, rows, :] = moved[:, :HD]
-            h_ref[h, rows, :] = h_ref[h, rows, :] + moved[:, HD:]
-
-
-def local_terms(q, k, v, beta, decay):
-    tokens = q.shape[0]
-    heads = 4
-    return pl.pallas_call(
-        local_kernel,
-        out_shape=(
-            jax.ShapeDtypeStruct((heads, HD, 2 * HD), STATE_TYPE),
-            jax.ShapeDtypeStruct((heads, tokens, HD), F32),
-            jax.ShapeDtypeStruct((heads, tokens, HD), F32),
-        ),
-        in_specs=[VMEM] * 6,
-        out_specs=(VMEM,) * 3,
-        scratch_shapes=[
-            pltpu.VMEM((heads, SPAN, tokens), F32),
-            pltpu.VMEM((heads, SPAN, tokens), F32),
-            pltpu.VMEM((heads, SPAN, tokens), F32),
-            pltpu.VMEM((heads, tokens, 2 * HD), F32),
-            pltpu.VMEM((heads, tokens, HD), F32),
-            pltpu.VMEM((heads, HD, tokens), F32),
-            pltpu.VMEM((8, 128), F32),
-            pltpu.VMEM((heads, tokens, HD), F32),
-            pltpu.VMEM((heads, tokens // SPAN, HD, 2 * HD), F32),
-            pltpu.VMEM((heads, tokens // SPAN, HD, 2 * HD), F32),
-        ],
-        compiler_params=params(),
-        name="local_terms",
-    )(q, k, v, beta, decay, decay.T)
-
-
-def along(dim, off):
-    at = [lax.axis_index(a) for a in AXES]
-    at[dim] = lax.rem(at[dim] + off, 4)
-    return tuple(at)
-
-
-def partner():
-    at = [lax.axis_index(a) for a in AXES]
-    at[3] = 1 - at[3]
-    return tuple(at)
-
-
-def greet(dims, pair):
-    barrier = pltpu.get_barrier_semaphore()
-    count = 0
-    for dim in dims:
-        for off in OFFSETS:
-            pl.semaphore_signal(barrier, inc=1, device_id=along(dim, off), device_id_type=MESH)
-            count += 1
-    if pair:
-        pl.semaphore_signal(barrier, inc=1, device_id=partner(), device_id_type=MESH)
-        count += 1
-    pl.semaphore_wait(barrier, count)
-
-
-def mixed_kernel(
-    map_ref, z_ref, h_ref, gate_ref, gain_ref, out_w_ref, residual_ref, norm_ref, meta_ref,
-    attended_ref, normed_ref, both_meta_ref,
-    row_s, plane_s, all_s, row_total, plane_total, state_out, state_in, mix_s, mix_in, acc_s,
-    send_sem, recv_sem,
-):
-    greet((0, 1, 2), True)
-    z, y, x, c = (lax.axis_index(a) for a in AXES)
+        map_s[h] = pre_s[blocks, h].astype(STATE_TYPE)
 
     def send(stage, dim, source, target):
         copies = []
@@ -263,23 +263,38 @@
             copy.start()
         return copies
 
-    def applied(step, carried):
+    def moved_by(step, carried):
         high, low = halves(carried)
-        moved = mm(step[:, :HD], high) + mm(step[:, :HD], low)
-        if carried.shape[1] == HD:
+        moved = mm(step[:, :HD], jnp.concatenate([high, low], 1))
+        width = carried.shape[1]
+        moved = moved[:, :width] + moved[:, width:]
+        if width == HD:
             return moved + step[:, HD:].astype(F32)
         return jnp.concatenate([moved[:, :HD], moved[:, HD:] + step[:, HD:].astype(F32)], 1)
 
     def total(steps):
         carried = steps[0].astype(F32)
         for i in range(1, 4):
-            carried = applied(steps[i], carried)
+            carried = moved_by(steps[i], carried)
         return carried.astype(STATE_TYPE)
 
+    def outputs(h):
+        z_s[h, 0:SPAN, :] = qp_s[h, 0:SPAN, :]
+        for n in range(1, blocks):
+            rows = slice(SPAN * n, SPAN * n + SPAN)
+            moved = mm2(halves(qp_s[h, rows, :]), pre_s[n, h].astype(BF16))
+            z_s[h, rows, :] = moved[:, :HD]
+            h_s[h, rows, :] = h_s[h, rows, :] + moved[:, HD:]
+
+    def light(h):
+        lanes = slice(h * HD, h * HD + HD)
+        lit_s[:, lanes] = silu(gate_s[:, lanes].astype(F32)) * gain_ref[...]
+
     sent = []
-    copies = send(0, 2, lambda t: map_ref.at[t], row_s)
+    pl.semaphore_wait(pltpu.get_barrier_semaphore(), greeted)
+    copies = send(0, 2, lambda t: map_s.at[t], rows_in)
     tell = pltpu.make_async_remote_copy(
-        src_ref=meta_ref,
+        src_ref=meta_s,
         dst_ref=both_meta_ref.at[c],
         send_sem=send_sem.at[4, 2],
         recv_sem=recv_sem.at[4, 2],
@@ -287,31 +302,36 @@
         device_id_type=MESH,
     )
     tell.start()
-    both_meta_ref[c] = meta_ref[...]
-    row_s[x] = map_ref[x]
+    both_meta_ref[c] = meta_s[...]
+    rows_in[x] = map_s[x]
+    for h in range(heads):
+        outputs(h)
     for copy in copies:
         copy.wait_recv()
     sent += copies
-    row_total[...] = total(row_s)
-    copies = send(1, 1, lambda t: row_total, plane_s)
-    plane_s[y] = row_total[...]
+    row_total[...] = total(rows_in)
+    copies = send(1, 1, lambda t: row_total, plane_in)
+    plane_in[y] = row_total[...]
+    loads[0].wait()
+    for h in range(heads):
+        light(h)
     for copy in copies:
         copy.wait_recv()
     sent += copies
-    plane_total[...] = total(plane_s)
-    copies = send(2, 0, lambda t: plane_total, all_s)
-    all_s[z] = plane_total[...]
+    plane_total[...] = total(plane_in)
+    copies = send(2, 0, lambda t: plane_total, all_in)
+    all_in[z] = plane_total[...]
     for copy in copies:
         copy.wait_recv()
     sent += copies
-    state = jnp.where(z > 0, all_s[0, :, HD:].astype(F32), 0.0)
+    state = jnp.where(z > 0, all_in[0, :, HD:].astype(F32), 0.0)
     for i in range(1, 3):
-        state = jnp.where(i < z, applied(all_s[i], state), state)
+        state = jnp.where(i < z, moved_by(all_in[i], state), state)
     for i in range(3):
-        state = jnp.where(i < y, applied(plane_s[i], state), state)
+        state = jnp.where(i < y, moved_by(plane_in[i], state), state)
     state_out[0] = state.astype(STATE_TYPE)
     for i in range(3):
-        state = applied(row_s[i], state)
+        state = moved_by(rows_in[i], state)
         state_out[i + 1] = state.astype(STATE_TYPE)
     copies = send(3, 2, lambda t: state_out.at[t], state_in)
     state_in[x] = state_out[x]
@@ -319,15 +339,12 @@
         copy.wait_recv()
     sent += copies
 
-    gain = gain_ref[...]
-    for h in range(4):
-        high, low = halves(z_ref[h])
-        state = state_in[h]
-        mix = h_ref[h] + mm(high, state) + mm(low, state)
-        mix = mix * lax.rsqrt(jnp.mean(mix * mix, axis=-1, keepdims=True) + EPS) * gain
-        mix = mix * silu(gate_ref[:, h * HD : h * HD + HD].astype(F32))
-        mix_s[:, h * HD : h * HD + HD] = mix.astype(BF16)
-    half = mix_s.shape[0] // 2
+    for h in range(heads):
+        lanes = slice(h * HD, h * HD + HD)
+        mix = h_s[h] + mm2(halves(z_s[h]), state_in[h])
+        mix = mix * lax.rsqrt(jnp.mean(mix * mix, axis=-1, keepdims=True) + EPS) * lit_s[:, lanes]
+        mix_s[:, lanes] = mix.astype(BF16)
+    half = tokens // 2
     width = mix_s.shape[1]
     other = 1 - c
     swap = pltpu.make_async_remote_copy(
@@ -339,18 +356,20 @@
         device_id_type=MESH,
     )
     swap.start()
+    for load in loads[1:]:
+        load.wait()
     own = pl.ds(pl.multiple_of(c * half, half), half)
     own_w = pl.ds(pl.multiple_of(c * width, width), width)
     other_w = pl.ds(pl.multiple_of(other * width, width), width)
-    model = out_w_ref.shape[1]
+    model = out_w_s.shape[1]
     for n in range(model // 512):
         cols = slice(512 * n, 512 * n + 512)
-        acc_s[:, cols] = residual_ref[:, cols].astype(F32) + mm(mix_s[own, :], out_w_ref[own_w, cols])
+        acc_s[:, cols] = residual_s[:, cols].astype(F32) + mm(mix_s[own, :], out_w_s[own_w, cols])
     swap.wait()
     squares = jnp.zeros((half, 1), F32)
     for n in range(model // 512):
         cols = slice(512 * n, 512 * n + 512)
-        piece = acc_s[:, cols] + mm(mix_in[...], out_w_ref[other_w, cols])
+        piece = acc_s[:, cols] + mm(mix_in[...], out_w_s[other_w, cols])
         piece = piece.astype(BF16)
         attended_ref[:, cols] = piece
         wide = piece.astype(F32)
@@ -375,34 +394,60 @@
         copy.wait_send()
 
 
-def mixed(maps, z, h, gate, gain, out_w, residual, norm_gain, meta):
+def attention(q, k, v, strength, inputs, extra, rate, gate, gain, out_w, residual, norm_gain, ids, weight):
     half, model = residual.shape
+    tokens, heads, blocks = 2 * half, 4, 2 * half // SPAN
+    hbm = pl.BlockSpec(memory_space=pl.ANY)
+    per_head = pltpu.VMEM((heads, tokens, HD), F32)
+    side = pltpu.VMEM((heads, SPAN, tokens), F32)
+    maps = pltpu.VMEM((4, HD, 2 * HD), STATE_TYPE)
     return pl.pallas_call(
-        mixed_kernel,
+        attention_kernel,
         out_shape=(
             jax.ShapeDtypeStruct((half, model), BF16),
-            jax.ShapeDtypeStruct((2 * half, model), BF16),
-            jax.ShapeDtypeStruct((2,) + meta.shape, F32),
+            jax.ShapeDtypeStruct((tokens, model), BF16),
+            jax.ShapeDtypeStruct((2, 2 * TOP_K, half), F32),
         ),
-        in_specs=[VMEM] * 9,
+        in_specs=[VMEM] * 7 + [hbm, VMEM, hbm, hbm] + [VMEM] * 3,
         out_specs=(VMEM,) * 3,
         scratch_shapes=[
-            pltpu.VMEM((4, HD, 2 * HD), STATE_TYPE),
-            pltpu.VMEM((4, HD, 2 * HD), STATE_TYPE),
-            pltpu.VMEM((4, HD, 2 * HD), STATE_TYPE),
+            per_head,
+            per_head,
+            pltpu.VMEM((8, tokens), F32),
+            side,
+            side,
+            side,
+            pltpu.VMEM((heads, tokens, 2 * HD), BF16),
+            per_head,
+            pltpu.VMEM((heads, HD, tokens), F32),
+            per_head,
+            pltpu.VMEM((heads, blocks, HD, 2 * HD), F32),
+            pltpu.VMEM((blocks + 1, heads, HD, 2 * HD), F32),
+            per_head,
+            per_head,
+            maps,
+            pltpu.VMEM((2 * TOP_K, half), F32),
+            pltpu.VMEM((tokens, heads * HD), BF16),
+            pltpu.VMEM((2 * heads * HD, model), BF16),
+            pltpu.VMEM((half, model), BF16),
+            pltpu.VMEM((tokens, heads * HD), F32),
+            maps,
+            maps,
+            maps,
             pltpu.VMEM((HD, 2 * HD), STATE_TYPE),
             pltpu.VMEM((HD, 2 * HD), STATE_TYPE),
             pltpu.VMEM((4, HD, HD), STATE_TYPE),
             pltpu.VMEM((4, HD, HD), STATE_TYPE),
-            pltpu.VMEM((2 * half, 4 * HD), BF16),
-            pltpu.VMEM((half, 4 * HD), BF16),
+            pltpu.VMEM((tokens, heads * HD), BF16),
+            pltpu.VMEM((half, heads * HD), BF16),
             pltpu.VMEM((half, model), F32),
             pltpu.SemaphoreType.DMA((5, 3)),
             pltpu.SemaphoreType.DMA((5, 3)),
+            pltpu.SemaphoreType.DMA((3,)),
         ],
         compiler_params=params(collective_id=0, has_side_effects=True),
-        name="mixed",
-    )(maps, z, h, gate, gain, out_w, residual, norm_gain, meta)
+        name="attention",
+    )(q, k, v, strength, inputs, extra, rate, gate, gain, out_w, residual, norm_gain, ids, weight)
 
 
 def at(ref, fixed):
@@ -727,22 +772,21 @@
     common_up_weight,
     common_down_weight,
 ):
-    beta = jax.nn.sigmoid(write_strength_logits.astype(F32))
-    decay = extra_log_decay - jnp.exp(head_rate_logarithm)[None, :] * jax.nn.softplus(
-        decay_input_logits.astype(F32) - 6.0
-    )
-    meta = jnp.concatenate([selected_expert_index.T.astype(F32), routing_weight.T], 0)
-    maps, z, h = local_terms(projected_queries, projected_keys, projected_values, beta, decay)
-    attended, normed, meta = mixed(
-        maps,
-        z,
-        h,
+    attended, normed, meta = attention(
+        projected_queries,
+        projected_keys,
+        projected_values,
+        write_strength_logits.T,
+        decay_input_logits.T,
+        extra_log_decay.T,
+        head_rate_logarithm[None, :],
         output_gate_values,
         per_head_norm_gain[None, :],
         output_matrix,
         residual,
         mixture_norm_gain[None, :],
-        meta,
+        selected_expert_index.T,
+        routing_weight.T,
     )
     return run_experts(
         normed,

time: 223 us -> 207 us (0.928)
  Pallas kernels: 215 us -> 204 us
  other arithmetic: 3.52 us -> 0 us
  local copies, waits for them, and re-layouts: 4.68 us -> 2.3 us
    pallas_call x2 -> x1, Pallas kernels: 59.6 us -> 49 us  [attention(): pl.pallas_call(attention_kernel, out_shape=(jax.ShapeDtypeStruct((half, m...]
where the time goes in v3:
time: 207 us
  Pallas kernels  204 us (99%)
  local copies, waits for them, and re-layouts  2.3 us (1%)
    pallas_call x1, Pallas kernels, run_experts(): pl.pallas_call(experts_kernel, out_shape=jax.ShapeDtypeStruct((half, mode...  155 us
    pallas_call x1, Pallas kernels, attention(): pl.pallas_call(attention_kernel, out_shape=(jax.ShapeDtypeStruct((half, m...  49 us

profile of v3, /device:TPU:1, one launch (start us, length us, event | category | flops | bytes accessed | tf_op | source)
XLA Modules:
  0.0 206.6 jit_solution(14124391137492969435)
XLA Ops:
  0.0 49.0 %attention.1 = (bf16[256,2048]{1,0:T(8,128)(2,1)}, bf16[512,2048]{1,0:T(8,128)(2,1)}, f32[2,8,256]{2,1,0:T(8,128)}) custom-call(bf16[512,512]{1,0:T(8,128)(2,1)} %q_ref.1, bf16[512,512]{1,0:T(8,128)(2,1)} %k_ref.1, bf16[512,512]{1,0:T(8,128)(2,1)} %v_ref.1, bf16[4,512]{1,0:T(4,128)(2,1)} %bitcast.16, bf16[4,512]{1,0:T(4,128)(2,1)} %bitcast.17, ...), custom_call_target="tpu_custom_call" | custom-call | tf_op jit(solution)/shard_map/attention/pallas_call | solution.py:404
  49.0 155.3 %experts.1 = bf16[256,2048]{1,0:T(8,128)(2,1)} custom-call(bf16[512,2048]{1,0:T(8,128)(2,1)} %get-tuple-element.8.normed_ref, bf16[256,2048]{1,0:T(8,128)(2,1)} %get-tuple-element.9.attended_ref, f32[2,8,256]{2,1,0:T(8,128)} %get-tuple-element.10.meta_ref, bf16[2048,512]{1,0:T(8,128)(2,1)} %bitcast.11, bf16[2048,512]{1,0:T(8,128)(2,1)} %bitcast.12, ...), custom_call_target="tpu_custom_call" | custom-call | tf_op jit(solution)/shard_map/experts/pallas_call | solution.py:726
  204.3 2.3 %copy.22 = bf16[256,2048]{1,0:T(8,128)(2,1)} copy(bf16[256,2048]{1,0:T(8,128)(2,1)} %experts.1) | data formatting | bytes 2097152

commit v4 on v3

--- a/solution.py
+++ b/solution.py
@@ -45,12 +45,14 @@
 
 def mm2(a, b, dims=((1,), (0,))):
     rows = a[0].shape[0]
+    if a[0].shape[1] == HD:
+        return mm(jnp.concatenate(a, 1), jnp.concatenate([b, b], dims[1][0]), dims)
     both = mm(jnp.concatenate(a, 0), b, dims)
     return both[:rows] + both[rows:]
 
 
 def silu(x):
-    return x / (1.0 + jnp.exp(-x))
+    return (0.5 * x) * (1.0 + jnp.tanh(0.5 * x))
 
 
 def iota(shape, dim):
@@ -89,10 +91,10 @@
 def attention_kernel(
     q_ref, k_ref, v_ref, strength_ref, input_ref, extra_ref, rate_ref, gate_hbm, gain_ref, out_w_hbm, residual_hbm,
     norm_ref, ids_ref, weight_ref,
-    attended_ref, normed_ref, both_meta_ref,
-    beta_s, g_s, row_s, low_s, score_s, inv_s, right_s, qd_s, kdt_s, qp_s, step_s, pre_s, z_s, h_s, map_s, meta_s,
+    attended_ref, normed_ref, both_meta_ref, code_ref,
+    beta_s, g_s, row_s, low_s, score_s, inv_s, right_s, qd_s, kdt_s, qp_s, step_s, pair_s, pre_s, span_s, z_s, h_s, map_s, meta_s,
     gate_s, out_w_s, residual_s, lit_s, rows_in, plane_in, all_in, row_total, plane_total, state_out, state_in,
-    mix_s, mix_in, acc_s, send_sem, recv_sem, load_sem,
+    mix_s, mix_in, acc_s, send_sem, recv_sem, share_send, share_recv, load_sem,
 ):
     heads, tokens = 4, q_ref.shape[0]
     blocks = tokens // SPAN
@@ -185,8 +187,8 @@
     def times2(a, b):
         return mm2(a, diag4(b.astype(BF16)))
 
-    def invert(part, _):
-        mine = [(2 * part + i // 2, slice(256 * (i % 2), 256 * (i % 2) + 256)) for i in range(4)]
+    def invert():
+        mine = [(i // 2, slice(256 * (i % 2), 256 * (i % 2) + 256)) for i in range(8)]
         lows = [low_s[h, :, s] for h, s in mine]
         small = r4 // 8 == p4 // 8
         d1 = [jnp.where(small, x, 0.0) for x in lows]
@@ -202,9 +204,8 @@
             inv = [x - times2(halves(x), e) for x, e in zip(inv, ex)]
         for (h, s), x in zip(mine, inv):
             inv_s[h, :, s] = x
-        return 0
-
-    lax.fori_loop(0, 2, invert, 0)
+
+    invert()
 
     def diag2(x):
         return jnp.concatenate([x * m for m in pair_masks], 0)
@@ -231,19 +232,21 @@
 
     lax.fori_loop(0, heads, apply, 0)
 
+    def compose(later, earlier):
+        moved = mm3(halves(later[:, :HD]), halves(earlier))
+        return jnp.concatenate([moved[:, :HD], moved[:, HD:] + later[:, HD:]], 1)
+
+    def pairs(i, _):
+        for h in range(heads):
+            pair_s[i, h] = compose(step_s[h, 2 * i + 1], step_s[h, 2 * i])
+        return 0
+
+    lax.fori_loop(0, 4, pairs, 0)
     for h in range(heads):
-        pre_s[1, h] = step_s[h, 0]
-
-    def grow(n, _):
-        for h in range(heads):
-            moved = mm3(halves(step_s[h, n, :, :HD]), halves(pre_s[n, h]))
-            pre_s[n + 1, h, :, :HD] = moved[:, :HD]
-            pre_s[n + 1, h, :, HD:] = moved[:, HD:] + step_s[h, n, :, HD:]
-        return 0
-
-    lax.fori_loop(1, blocks, grow, 0)
+        pre_s[4, h] = compose(pair_s[1, h], pair_s[0, h])
+        pair_s[4, h] = compose(pair_s[3, h], pair_s[2, h])
     for h in range(heads):
-        map_s[h] = pre_s[blocks, h].astype(STATE_TYPE)
+        map_s[h] = compose(pair_s[4, h], pre_s[4, h]).astype(STATE_TYPE)
 
     def send(stage, dim, source, target):
         copies = []
@@ -259,8 +262,8 @@
                     device_id_type=MESH,
                 )
             )
-        for copy in copies:
-            copy.start()
+        for n in (2, 0, 1):
+            copies[n].start()
         return copies
 
     def moved_by(step, carried):
@@ -272,13 +275,13 @@
             return moved + step[:, HD:].astype(F32)
         return jnp.concatenate([moved[:, :HD], moved[:, HD:] + step[:, HD:].astype(F32)], 1)
 
-    def total(steps):
-        carried = steps[0].astype(F32)
-        for i in range(1, 4):
-            carried = moved_by(steps[i], carried)
-        return carried.astype(STATE_TYPE)
-
     def outputs(h):
+        pre_s[1, h] = step_s[h, 0]
+        pre_s[2, h] = pair_s[0, h]
+        pre_s[3, h] = compose(step_s[h, 2], pair_s[0, h])
+        pre_s[5, h] = compose(step_s[h, 4], pre_s[4, h])
+        pre_s[6, h] = compose(pair_s[2, h], pre_s[4, h])
+        pre_s[7, h] = compose(step_s[h, 6], pre_s[6, h])
         z_s[h, 0:SPAN, :] = qp_s[h, 0:SPAN, :]
         for n in range(1, blocks):
             rows = slice(SPAN * n, SPAN * n + SPAN)
@@ -309,30 +312,56 @@
     for copy in copies:
         copy.wait_recv()
     sent += copies
-    row_total[...] = total(rows_in)
+    low_pair = moved_by(rows_in[1], rows_in[0].astype(F32))
+    high_pair = moved_by(rows_in[3], rows_in[2].astype(F32))
+    span_s[2] = low_pair
+    row_total[...] = compose(high_pair, low_pair).astype(STATE_TYPE)
     copies = send(1, 1, lambda t: row_total, plane_in)
     plane_in[y] = row_total[...]
+    span_s[1] = rows_in[0].astype(F32)
+    span_s[3] = moved_by(rows_in[2], span_s[2])
     loads[0].wait()
     for h in range(heads):
         light(h)
     for copy in copies:
         copy.wait_recv()
     sent += copies
-    plane_total[...] = total(plane_in)
+    low_pair = moved_by(plane_in[1], plane_in[0].astype(F32))
+    high_pair = moved_by(plane_in[3], plane_in[2].astype(F32))
+    plane_total[...] = compose(high_pair, low_pair).astype(STATE_TYPE)
     copies = send(2, 0, lambda t: plane_total, all_in)
     all_in[z] = plane_total[...]
+    entry = jnp.where(y == 1, plane_in[0].astype(F32), jnp.concatenate([eye, jnp.zeros((HD, HD), F32)], 1))
+    entry = jnp.where(y == 2, low_pair, entry)
+    entry = jnp.where(y == 3, moved_by(plane_in[2], low_pair), entry)
+    span_s[0] = entry
+    for i in range(1, 4):
+        span_s[i] = compose(span_s[i], entry)
+
+    tell.wait()
+    chips = code_ref.shape[0]
+    expert = (2 * iota((chips, 1), 0) + c).astype(F32)
+    chosen = jnp.zeros((chips, tokens), F32)
+    for j in range(TOP_K):
+        ids = jnp.concatenate([both_meta_ref[0, j : j + 1, :], both_meta_ref[1, j : j + 1, :]], 1)
+        chosen = chosen + jnp.where(ids == expert, 1.0, 0.0)
+    i512, j512 = iota((tokens, tokens), 0), iota((tokens, tokens), 1)
+    half = tokens // 2
+    before = jnp.where((i512 // half == j512 // half) & (i512 < j512), 1.0, 0.0).astype(BF16)
+    slot = mm(chosen.astype(BF16), before)
+    shift = jnp.where(iota((chips, tokens), 1) < half, 0.0, float(CAP))
+    code_ref[...] = jnp.where(chosen > 0.0, slot + shift, -1.0)
+
     for copy in copies:
         copy.wait_recv()
     sent += copies
     state = jnp.where(z > 0, all_in[0, :, HD:].astype(F32), 0.0)
     for i in range(1, 3):
         state = jnp.where(i < z, moved_by(all_in[i], state), state)
-    for i in range(3):
-        state = jnp.where(i < y, moved_by(plane_in[i], state), state)
-    state_out[0] = state.astype(STATE_TYPE)
-    for i in range(3):
-        state = moved_by(rows_in[i], state)
-        state_out[i + 1] = state.astype(STATE_TYPE)
+    state = halves(state)
+    for i in range(4):
+        entering = mm3(halves(span_s[i, :, :HD]), state) + span_s[i, :, HD:]
+        state_out[i] = entering.astype(STATE_TYPE)
     copies = send(3, 2, lambda t: state_out.at[t], state_in)
     state_in[x] = state_out[x]
     for copy in copies:
@@ -344,7 +373,6 @@
         mix = h_s[h] + mm2(halves(z_s[h]), state_in[h])
         mix = mix * lax.rsqrt(jnp.mean(mix * mix, axis=-1, keepdims=True) + EPS) * lit_s[:, lanes]
         mix_s[:, lanes] = mix.astype(BF16)
-    half = tokens // 2
     width = mix_s.shape[1]
     other = 1 - c
     swap = pltpu.make_async_remote_copy(
@@ -376,20 +404,22 @@
         acc_s[:, cols] = wide
         squares = squares + jnp.sum(wide * wide, axis=-1, keepdims=True)
     scale = lax.rsqrt(squares / model + EPS)
+    shares = []
     for n in range(model // 512):
         cols = slice(512 * n, 512 * n + 512)
         normed_ref[own, cols] = (acc_s[:, cols] * scale * norm_ref[:, cols]).astype(BF16)
-    share = pltpu.make_async_remote_copy(
-        src_ref=normed_ref.at[own],
-        dst_ref=normed_ref.at[own],
-        send_sem=send_sem.at[4, 1],
-        recv_sem=recv_sem.at[4, 1],
-        device_id=partner(),
-        device_id_type=MESH,
-    )
-    share.start()
-    tell.wait()
-    share.wait()
+        share = pltpu.make_async_remote_copy(
+            src_ref=normed_ref.at[own, cols],
+            dst_ref=normed_ref.at[own, cols],
+            send_sem=share_send.at[n],
+            recv_sem=share_recv.at[n],
+            device_id=partner(),
+            device_id_type=MESH,
+        )
+        share.start()
+        shares.append(share)
+    for share in shares:
+        share.wait()
     for copy in sent:
         copy.wait_send()
 
@@ -407,9 +437,10 @@
             jax.ShapeDtypeStruct((half, model), BF16),
             jax.ShapeDtypeStruct((tokens, model), BF16),
             jax.ShapeDtypeStruct((2, 2 * TOP_K, half), F32),
+            jax.ShapeDtypeStruct((64, tokens), F32),
         ),
         in_specs=[VMEM] * 7 + [hbm, VMEM, hbm, hbm] + [VMEM] * 3,
-        out_specs=(VMEM,) * 3,
+        out_specs=(VMEM,) * 4,
         scratch_shapes=[
             per_head,
             per_head,
@@ -422,7 +453,9 @@
             pltpu.VMEM((heads, HD, tokens), F32),
             per_head,
             pltpu.VMEM((heads, blocks, HD, 2 * HD), F32),
-            pltpu.VMEM((blocks + 1, heads, HD, 2 * HD), F32),
+            pltpu.VMEM((5, heads, HD, 2 * HD), F32),
+            pltpu.VMEM((blocks, heads, HD, 2 * HD), F32),
+            pltpu.VMEM((4, HD, 2 * HD), F32),
             per_head,
             per_head,
             maps,
@@ -443,6 +476,8 @@
             pltpu.VMEM((half, model), F32),
             pltpu.SemaphoreType.DMA((5, 3)),
             pltpu.SemaphoreType.DMA((5, 3)),
+            pltpu.SemaphoreType.DMA((4,)),
+            pltpu.SemaphoreType.DMA((4,)),
             pltpu.SemaphoreType.DMA((3,)),
         ],
         compiler_params=params(collective_id=0, has_side_effects=True),
@@ -455,10 +490,10 @@
 
 
 def experts_kernel(
-    normed_ref, attended_ref, meta_ref, gate_hbm, up_hbm, down_hbm, common_gate_hbm, common_up_hbm, common_down_hbm,
+    normed_ref, attended_hbm, meta_ref, code_ref, gate_hbm, up_hbm, down_hbm, common_gate_hbm, common_up_hbm, common_down_hbm,
     out_ref,
     buf0, buf1, buf2, buf3, buf4, gate_w, up_w, down_w, common_gate_w, common_up_w, common_down_w,
-    code_s, pick_s, acc_s, away_s, here_s,
+    attended_s, pick_s, acc_s, away_s, here_s,
     send1, recv1, send2, recv2, send3, recv3, free_sem, swap_send, swap_recv, load_sem,
 ):
     tokens, model = normed_ref.shape
@@ -469,6 +504,7 @@
         pltpu.make_async_copy(a, b, load_sem.at[i])
         for i, (a, b) in enumerate(
             (
+                (attended_hbm, attended_s),
                 (common_gate_hbm, common_gate_w),
                 (common_up_hbm, common_up_w),
                 (common_down_hbm, common_down_w),
@@ -560,44 +596,30 @@
         place = coord[d2] if m == 0 else back[d2][m - 1]
         keep(at(bufs[2].at[k], {d2: place, d3: coord[d3]}), at(bufs[3].at[k], {d2: place, d3: coord[d3]}))
 
-    expert = (2 * iota((chips, 1), 0) + c).astype(F32)
-    chosen = jnp.zeros((chips, tokens), F32)
-    for j in range(TOP_K):
-        ids = jnp.concatenate([meta_ref[0, j : j + 1, :], meta_ref[1, j : j + 1, :]], 1)
-        chosen = chosen + jnp.where(ids == expert, 1.0, 0.0)
-    i, j = iota((tokens, tokens), 0), iota((tokens, tokens), 1)
-    same = i // half == j // half
-    before = jnp.where(same & (i < j), 1.0, 0.0).astype(BF16)
-    slot = mm(chosen.astype(BF16), before)
-    shift = jnp.where(iota((chips, tokens), 1) < half, 0.0, float(CAP))
-    code_s[...] = jnp.where(chosen > 0.0, slot + shift, -1.0)
     greet((0, 1, 2), True)
-    for k in range(3):
+    for k in (0, 2, 1):
         low = 0 if k < 2 else half
         high = half if k == 0 else tokens
-
-        def one(zi, _):
-            code = code_s[pl.ds(pl.multiple_of(zi * 16, 16), 16), low:high]
-            wanted = (iota((16, 8, high - low), 1) + 8 * k).astype(F32)
-            pick = jnp.where(code[:, None, :] == wanted, 1.0, 0.0).reshape(128, high - low).astype(BF16)
-            rows = mm(pick, normed_ref[low:high, :]).astype(BF16)
-            buf0[k, zi] = rows.reshape(4, 4, 8, model)
-            return 0
-
-        lax.fori_loop(0, 4, one, 0)
+        wanted = (iota((chips, 8, high - low), 1) + 8 * k).astype(F32)
+        pick = jnp.where(code_ref[:, low:high][:, None, :] == wanted, 1.0, 0.0)
+        pick = pick.reshape(8 * chips, high - low).astype(BF16)
+        for n in range(model // 512):
+            cols = slice(512 * n, 512 * n + 512)
+            rows = mm(pick, normed_ref[low:high, cols]).astype(BF16)
+            buf0[k, :, :, :, :, cols] = rows.reshape(4, 4, 4, 8, 512)
         for n in range(3):
             first(0, k, n).start()
     for k in range(3):
         start_second(0, k, 0)
 
-    for load in loads[:3]:
+    for load in loads[:4]:
         load.wait()
     own = pl.ds(pl.multiple_of(c * half, half), half)
     hidden = silu(mm(normed_ref[own, :], common_gate_w[...])) * mm(normed_ref[own, :], common_up_w[...])
     hidden = hidden.astype(BF16)
     for n in range(model // 512):
         cols = slice(512 * n, 512 * n + 512)
-        acc_s[:, cols] = attended_ref[:, cols].astype(F32) + mm(hidden, common_down_w[:, cols])
+        acc_s[:, cols] = attended_s[:, cols].astype(F32) + mm(hidden, common_down_w[:, cols])
 
     for n in range(3):
         for k in range(3):
@@ -614,7 +636,8 @@
         hit = meta[:, q : q + 1] == expert
         chosen = chosen + jnp.where(hit, 1.0, 0.0)
         weight = weight + jnp.where(hit, meta[:, TOP_K + q : TOP_K + q + 1], 0.0)
-    before = jnp.where(same & (j < i), 1.0, 0.0).astype(BF16)
+    i, j = iota((tokens, tokens), 0), iota((tokens, tokens), 1)
+    before = jnp.where((i // half == j // half) & (j < i), 1.0, 0.0).astype(BF16)
     slot = mm(before, chosen.astype(BF16))
     shift = jnp.where(iota((tokens, chips), 0) < half, 0.0, float(CAP))
     code = jnp.where(chosen > 0.0, slot + shift, -1.0).astype(BF16)
@@ -640,7 +663,7 @@
         for off in OFFSETS:
             pl.semaphore_signal(free_sem.at[0, k], inc=1, device_id=along(d2, off), device_id_type=MESH)
             pl.semaphore_signal(free_sem.at[1, k], inc=1, device_id=along(d1, off), device_id_type=MESH)
-    for load in loads[3:]:
+    for load in loads[4:]:
         load.wait()
 
     def serve(places):
@@ -719,19 +742,19 @@
             first(1, k, n).wait_send()
 
 
-def run_experts(normed, attended, meta, gate, up, down, common_gate, common_up, common_down):
+def run_experts(normed, attended, meta, code, gate, up, down, common_gate, common_up, common_down):
     half, model = attended.shape
     buffer = pltpu.VMEM((3, 4, 4, 4, 8, model), BF16)
     hbm = pl.BlockSpec(memory_space=pl.ANY)
     return pl.pallas_call(
         experts_kernel,
         out_shape=jax.ShapeDtypeStruct((half, model), BF16),
-        in_specs=[VMEM] * 3 + [hbm] * 6,
+        in_specs=[VMEM, hbm, VMEM, VMEM] + [hbm] * 6,
         out_specs=VMEM,
         scratch_shapes=[buffer] * 5
         + [pltpu.VMEM(w.shape, BF16) for w in (gate, up, down, common_gate, common_up, common_down)]
         + [
-            pltpu.VMEM((64, 2 * half), F32),
+            pltpu.VMEM((half, model), BF16),
             pltpu.VMEM((3, 2 * half, 512), BF16),
             pltpu.VMEM((half, model), F32),
             pltpu.VMEM((model // 512, half, 512), F32),
@@ -743,11 +766,11 @@
             pltpu.SemaphoreType.REGULAR((2, 3)),
             pltpu.SemaphoreType.DMA((model // 512,)),
             pltpu.SemaphoreType.DMA((model // 512,)),
-            pltpu.SemaphoreType.DMA((6,)),
+            pltpu.SemaphoreType.DMA((7,)),
         ],
         compiler_params=params(collective_id=1, has_side_effects=True),
         name="experts",
-    )(normed, attended, meta, gate, up, down, common_gate, common_up, common_down)
+    )(normed, attended, meta, code, gate, up, down, common_gate, common_up, common_down)
 
 
 def shards(
@@ -772,7 +795,7 @@
     common_up_weight,
     common_down_weight,
 ):
-    attended, normed, meta = attention(
+    attended, normed, meta, code = attention(
         projected_queries,
         projected_keys,
         projected_values,
@@ -792,6 +815,7 @@
         normed,
         attended,
         meta,
+        code,
         routed_gate_weight[0],
         routed_up_weight[0],
         routed_down_weight[0],

time: 207 us -> 200 us (0.966)
  Pallas kernels: 204 us -> 198 us
    pallas_call x1, Pallas kernels: 49 us -> 44.7 us  [attention(): pl.pallas_call(attention_kernel, out_shape=(jax.ShapeDtypeStruct((half, m...]
    pallas_call x1, Pallas kernels: 155 us -> 153 us  [run_experts(): pl.pallas_call(experts_kernel, out_shape=jax.ShapeDtypeStruct((half, mode...]
where the time goes in v4:
time: 200 us
  Pallas kernels  198 us (99%)
  local copies, waits for them, and re-layouts  2.3 us (1%)
    pallas_call x1, Pallas kernels, run_experts(): pl.pallas_call(experts_kernel, out_shape=jax.ShapeDtypeStruct((half, mode...  153 us
    pallas_call x1, Pallas kernels, attention(): pl.pallas_call(attention_kernel, out_shape=(jax.ShapeDtypeStruct((half, m...  44.7 us

profile of v4, /device:TPU:1, one launch (start us, length us, event | category | flops | bytes accessed | tf_op | source)
XLA Modules:
  0.0 200.2 jit_solution(13267075707724023316)
XLA Ops:
  0.0 44.7 %attention.1 = (bf16[256,2048]{1,0:T(8,128)(2,1)}, bf16[512,2048]{1,0:T(8,128)(2,1)}, f32[2,8,256]{2,1,0:T(8,128)}, f32[64,512]{1,0:T(8,128)}) custom-call(bf16[512,512]{1,0:T(8,128)(2,1)} %q_ref.1, bf16[512,512]{1,0:T(8,128)(2,1)} %k_ref.1, bf16[512,512]{1,0:T(8,128)(2,1)} %v_ref.1, bf16[4,512]{1,0:T(4,128)(2,1)} %bitcast.16, bf16[4,512]{1,0:T(4,128)(2,1)} %bitcast.17, ...), custom_call_target="tpu_custom_call" | custom-call | tf_op jit(solution)/shard_map/attention/pallas_call | solution.py:434
  44.7 153.1 %experts.1 = bf16[256,2048]{1,0:T(8,128)(2,1)} custom-call(bf16[512,2048]{1,0:T(8,128)(2,1)} %get-tuple-element.9.normed_ref, bf16[256,2048]{1,0:T(8,128)(2,1)} %get-tuple-element.10.attended_hbm, f32[2,8,256]{2,1,0:T(8,128)} %get-tuple-element.11.meta_ref, f32[64,512]{1,0:T(8,128)} %get-tuple-element.12.code_ref, bf16[2048,512]{1,0:T(8,128)(2,1)} %bitcast.11, ...), custom_call_target="tpu_custom_call" | custom-call | tf_op jit(solution)/shard_map/experts/pallas_call | solution.py:749
  197.9 2.3 %copy.22 = bf16[256,2048]{1,0:T(8,128)(2,1)} copy(bf16[256,2048]{1,0:T(8,128)(2,1)} %experts.1) | data formatting | bytes 2097152

commit v5 on v4

--- a/solution.py
+++ b/solution.py
@@ -71,10 +71,6 @@
     return tuple(at)
 
 
-def greet(dims, pair):
-    pl.semaphore_wait(pltpu.get_barrier_semaphore(), arrive(dims, pair))
-
-
 def arrive(dims, pair):
     barrier = pltpu.get_barrier_semaphore()
     count = 0
@@ -92,7 +88,7 @@
     q_ref, k_ref, v_ref, strength_ref, input_ref, extra_ref, rate_ref, gate_hbm, gain_ref, out_w_hbm, residual_hbm,
     norm_ref, ids_ref, weight_ref,
     attended_ref, normed_ref, both_meta_ref, code_ref,
-    beta_s, g_s, row_s, low_s, score_s, inv_s, right_s, qd_s, kdt_s, qp_s, step_s, pair_s, pre_s, span_s, z_s, h_s, map_s, meta_s,
+    beta_s, g_s, row_s, low_s, decay_s, inv_s, right_s, kk_s, wu_s, kdt_s, qp_s, step_s, pair_s, pre_s, span_s, z_s, h_s, map_s, meta_s,
     gate_s, out_w_s, residual_s, lit_s, rows_in, plane_in, all_in, row_total, plane_total, state_out, state_in,
     mix_s, mix_in, acc_s, send_sem, recv_sem, share_send, share_recv, load_sem,
 ):
@@ -144,8 +140,6 @@
 
     def prepare(h, _):
         lanes = pl.ds(pl.multiple_of(h * HD, HD), HD)
-        q = silu(q_ref[:, lanes].astype(F32))
-        q = q * lax.rsqrt(jnp.sum(q * q, axis=-1, keepdims=True) + EPS)
         k = silu(k_ref[:, lanes].astype(F32))
         k = k * lax.rsqrt(jnp.sum(k * k, axis=-1, keepdims=True) + EPS)
         v = silu(v_ref[:, lanes].astype(F32))
@@ -154,21 +148,20 @@
         kb = k * b_h
         right_s[h, :, :HD] = (kb * grown).astype(BF16)
         right_s[h, :, HD:] = (v * b_h).astype(BF16)
-        qd_s[h] = q * grown
         gr = row_s[pl.ds(h, 1), :]
         kdt_s[h] = k.T * jnp.exp(row_s[pl.ds(h + heads, 1), :] - gr)
-        ks, kbs, qs = halves(k), halves(kb), halves(q)
+        ks, kbs = halves(k), halves(kb)
+        kk_s[h, :, :HD] = ks[0]
+        kk_s[h, :, HD:] = ks[1]
         for j in range(tokens // 128):
             rows = slice(128 * j, 128 * j + 128)
-            left = tuple(jnp.concatenate([a[rows], b[rows]], 0) for a, b in zip(kbs, qs))
-            both = mm3(left, tuple(a[rows] for a in ks), ((1,), (1,)))
+            both = mm3(tuple(a[rows] for a in kbs), tuple(a[rows] for a in ks), ((1,), (1,)))
             inner = jnp.where(first, both[0:64], both[64:128])
-            score = jnp.where(first, both[128:192], both[192:256])
             gi = jnp.where(first, g_h[128 * j : 128 * j + 64], g_h[128 * j + 64 : 128 * j + 128])
             spread = jnp.where(causal, gi - gr[:, rows], 0.0)
             decay = jnp.where(causal, jnp.exp(spread), 0.0)
             low_s[h, :, rows] = jnp.where(strict, inner * decay, 0.0)
-            score_s[h, :, rows] = score * decay
+            decay_s[h, :, rows] = decay
         return 0
 
     lax.fori_loop(0, heads, prepare, 0)
@@ -215,14 +208,10 @@
             rows = slice(128 * j, 128 * j + 128)
             inv = tuple(diag2(x) for x in halves(inv_s[h, :, rows]))
             wu = mm2(inv, right_s[h, rows, :]).astype(BF16)
-            score = [diag2(x) for x in halves(score_s[h, :, rows])]
+            wu_s[h, rows, :] = wu
             kdt = kdt_s[h, :, rows]
             kdt = halves(jnp.concatenate([jnp.where(first_wide, kdt, 0.0), jnp.where(first_wide, 0.0, kdt)], 0))
-            left = tuple(jnp.concatenate([a, b], 0) for a, b in zip(score, kdt))
-            both = mm2(left, wu)
-            qp_s[h, rows, :] = qd_s[h, rows, :] - both[:128, :HD]
-            h_s[h, rows, :] = both[:128, HD:]
-            change = both[128:]
+            change = mm2(kdt, wu)
             for i in range(2):
                 n = 2 * j + i
                 factor = jnp.exp(g_s[h, n * SPAN + SPAN - 1 : n * SPAN + SPAN, :])
@@ -275,6 +264,22 @@
             return moved + step[:, HD:].astype(F32)
         return jnp.concatenate([moved[:, :HD], moved[:, HD:] + step[:, HD:].astype(F32)], 1)
 
+    def scores(h, _):
+        lanes = pl.ds(pl.multiple_of(h * HD, HD), HD)
+        q = silu(q_ref[:, lanes].astype(F32))
+        q = q * lax.rsqrt(jnp.sum(q * q, axis=-1, keepdims=True) + EPS)
+        qd = q * jnp.exp(g_s[h])
+        qs = halves(q)
+        for j in range(tokens // 128):
+            rows = slice(128 * j, 128 * j + 128)
+            ks = (kk_s[h, rows, :HD], kk_s[h, rows, HD:])
+            both = mm3(tuple(a[rows] for a in qs), ks, ((1,), (1,)))
+            score = jnp.where(first, both[0:64], both[64:128]) * decay_s[h, :, rows]
+            both = mm2(tuple(diag2(x) for x in halves(score)), wu_s[h, rows, :])
+            qp_s[h, rows, :] = qd[rows] - both[:, :HD]
+            h_s[h, rows, :] = both[:, HD:]
+        return 0
+
     def outputs(h):
         pre_s[1, h] = step_s[h, 0]
         pre_s[2, h] = pair_s[0, h]
@@ -307,8 +312,7 @@
     tell.start()
     both_meta_ref[c] = meta_s[...]
     rows_in[x] = map_s[x]
-    for h in range(heads):
-        outputs(h)
+    lax.fori_loop(0, heads, scores, 0)
     for copy in copies:
         copy.wait_recv()
     sent += copies
@@ -323,6 +327,7 @@
     loads[0].wait()
     for h in range(heads):
         light(h)
+        outputs(h)
     for copy in copies:
         copy.wait_recv()
     sent += copies
@@ -449,7 +454,8 @@
             side,
             side,
             pltpu.VMEM((heads, tokens, 2 * HD), BF16),
-            per_head,
+            pltpu.VMEM((heads, tokens, 2 * HD), BF16),
+            pltpu.VMEM((heads, tokens, 2 * HD), BF16),
             pltpu.VMEM((heads, HD, tokens), F32),
             per_head,
             pltpu.VMEM((heads, blocks, HD, 2 * HD), F32),
@@ -517,6 +523,7 @@
     for load in loads:
         load.start()
 
+    greeted = arrive((0, 1, 2), True)
     coord = [lax.axis_index(a) for a in SP]
     away = [[lax.rem(coord[d] + off, 4) for off in OFFSETS] for d in range(3)]
     back = [[lax.rem(coord[d] + 4 - off, 4) for off in OFFSETS] for d in range(3)]
@@ -596,7 +603,6 @@
         place = coord[d2] if m == 0 else back[d2][m - 1]
         keep(at(bufs[2].at[k], {d2: place, d3: coord[d3]}), at(bufs[3].at[k], {d2: place, d3: coord[d3]}))
 
-    greet((0, 1, 2), True)
     for k in (0, 2, 1):
         low = 0 if k < 2 else half
         high = half if k == 0 else tokens
@@ -607,6 +613,8 @@
             cols = slice(512 * n, 512 * n + 512)
             rows = mm(pick, normed_ref[low:high, cols]).astype(BF16)
             buf0[k, :, :, :, :, cols] = rows.reshape(4, 4, 4, 8, 512)
+        if k == 0:
+            pl.semaphore_wait(pltpu.get_barrier_semaphore(), greeted)
         for n in range(3):
             first(0, k, n).start()
     for k in range(3):

time: 200 us -> 199 us (level)
  Pallas kernels: 198 us -> 196 us
where the time goes in v5:
time: 199 us
  Pallas kernels  196 us (98%)
  local copies, waits for them, and re-layouts  2.3 us (1%)
    pallas_call x1, Pallas kernels, run_experts(): pl.pallas_call(experts_kernel, out_shape=jax.ShapeDtypeStruct((half, mode...  152 us
    pallas_call x1, Pallas kernels, attention(): pl.pallas_call(attention_kernel, out_shape=(jax.ShapeDtypeStruct((half, m...  43.9 us

profile of v5, /device:TPU:1, one launch (start us, length us, event | category | flops | bytes accessed | tf_op | source)
XLA Modules:
  0.0 198.6 jit_solution(5675072794286997742)
XLA Ops:
  0.0 43.9 %attention.1 = (bf16[256,2048]{1,0:T(8,128)(2,1)}, bf16[512,2048]{1,0:T(8,128)(2,1)}, f32[2,8,256]{2,1,0:T(8,128)}, f32[64,512]{1,0:T(8,128)}) custom-call(bf16[512,512]{1,0:T(8,128)(2,1)} %q_ref.1, bf16[512,512]{1,0:T(8,128)(2,1)} %k_ref.1, bf16[512,512]{1,0:T(8,128)(2,1)} %v_ref.1, bf16[4,512]{1,0:T(4,128)(2,1)} %bitcast.16, bf16[4,512]{1,0:T(4,128)(2,1)} %bitcast.17, ...), custom_call_target="tpu_custom_call" | custom-call | tf_op jit(solution)/shard_map/attention/pallas_call | solution.py:439
  43.9 152.4 %experts.1 = bf16[256,2048]{1,0:T(8,128)(2,1)} custom-call(bf16[512,2048]{1,0:T(8,128)(2,1)} %get-tuple-element.9.normed_ref, bf16[256,2048]{1,0:T(8,128)(2,1)} %get-tuple-element.10.attended_hbm, f32[2,8,256]{2,1,0:T(8,128)} %get-tuple-element.11.meta_ref, f32[64,512]{1,0:T(8,128)} %get-tuple-element.12.code_ref, bf16[2048,512]{1,0:T(8,128)(2,1)} %bitcast.11, ...), custom_call_target="tpu_custom_call" | custom-call | tf_op jit(solution)/shard_map/experts/pallas_call | solution.py:757
  196.3 2.3 %copy.22 = bf16[256,2048]{1,0:T(8,128)(2,1)} copy(bf16[256,2048]{1,0:T(8,128)(2,1)} %experts.1) | data formatting | bytes 2097152

commit v6 on v5

--- a/solution.py
+++ b/solution.py
@@ -19,7 +19,7 @@
 HIGH = lax.Precision.HIGHEST
 MESH = pl.DeviceIdType.MESH
 VMEM = pl.BlockSpec(memory_space=pltpu.VMEM)
-OFFSETS = (1, 3, 2)
+OFFSETS = (2, 1, 3)
 ORDERS = ((2, 1, 0), (1, 0, 2), (0, 2, 1))
 STATE_TYPE = BF16
 
@@ -251,7 +251,7 @@
                     device_id_type=MESH,
                 )
             )
-        for n in (2, 0, 1):
+        for n in range(3):
             copies[n].start()
         return copies
 
@@ -781,6 +781,40 @@
     )(normed, attended, meta, code, gate, up, down, common_gate, common_up, common_down)
 
 
+def settle_kernel(src_ref, dst_ref, held, in_sem, out_sem):
+    step = held.shape[1]
+    loads, stores = [], []
+    for i in range(held.shape[0]):
+        rows = slice(step * i, step * i + step)
+        loads.append(pltpu.make_async_copy(src_ref.at[rows], held.at[i], in_sem.at[i]))
+        stores.append(pltpu.make_async_copy(held.at[i], dst_ref.at[rows], out_sem.at[i]))
+    for load in loads:
+        load.start()
+    for load, store in zip(loads, stores):
+        load.wait()
+        store.start()
+    for store in stores:
+        store.wait()
+
+
+def settle(out):
+    rows, model = out.shape
+    hbm = pl.BlockSpec(memory_space=pl.ANY)
+    return pl.pallas_call(
+        settle_kernel,
+        out_shape=jax.ShapeDtypeStruct(out.shape, out.dtype),
+        in_specs=[hbm],
+        out_specs=hbm,
+        scratch_shapes=[
+            pltpu.VMEM((4, rows // 4, model), out.dtype),
+            pltpu.SemaphoreType.DMA((4,)),
+            pltpu.SemaphoreType.DMA((4,)),
+        ],
+        compiler_params=params(),
+        name="settle",
+    )(out)
+
+
 def shards(
     projected_queries,
     projected_keys,
@@ -819,7 +853,7 @@
         selected_expert_index.T,
         routing_weight.T,
     )
-    return run_experts(
+    out = run_experts(
         normed,
         attended,
         meta,
@@ -831,6 +865,7 @@
         common_up_weight,
         common_down_weight,
     )
+    return settle(out)
 
 
 def solution(mesh):

time: 199 us -> 199 us (level)
  local copies, waits for them, and re-layouts: 2.3 us -> 0 us
  Pallas kernels: 196 us -> 198 us
    unnamed x1 -> x0, local copies, waits for them, and re-layouts: 2.3 us -> none
where the time goes in v6:
time: 199 us; the launch traced here: 198 us
  Pallas kernels  198 us (99%)
    pallas_call x1, Pallas kernels, run_experts(): pl.pallas_call(experts_kernel, out_shape=jax.ShapeDtypeStruct((half, mode...  152 us
    pallas_call x1, Pallas kernels, attention(): pl.pallas_call(attention_kernel, out_shape=(jax.ShapeDtypeStruct((half, m...  43.9 us

profile of v6, /device:TPU:1, one launch (start us, length us, event | category | flops | bytes accessed | tf_op | source)
XLA Modules:
  0.0 198.4 jit_solution(13634717498027756918)
XLA Ops:
  0.0 43.9 %attention.1 = (bf16[256,2048]{1,0:T(8,128)(2,1)}, bf16[512,2048]{1,0:T(8,128)(2,1)}, f32[2,8,256]{2,1,0:T(8,128)}, f32[64,512]{1,0:T(8,128)}) custom-call(bf16[512,512]{1,0:T(8,128)(2,1)} %q_ref.1, bf16[512,512]{1,0:T(8,128)(2,1)} %k_ref.1, bf16[512,512]{1,0:T(8,128)(2,1)} %v_ref.1, bf16[4,512]{1,0:T(4,128)(2,1)} %bitcast.16, bf16[4,512]{1,0:T(4,128)(2,1)} %bitcast.17, ...), custom_call_target="tpu_custom_call" | custom-call | tf_op jit(solution)/shard_map/attention/pallas_call | solution.py:439
  43.9 152.4 %experts.1.src_ref = bf16[256,2048]{1,0:T(8,128)(2,1)} custom-call(bf16[512,2048]{1,0:T(8,128)(2,1)} %get-tuple-element.9.normed_ref, bf16[256,2048]{1,0:T(8,128)(2,1)} %get-tuple-element.10.attended_hbm, f32[2,8,256]{2,1,0:T(8,128)} %get-tuple-element.11.meta_ref, f32[64,512]{1,0:T(8,128)} %get-tuple-element.12.code_ref, bf16[2048,512]{1,0:T(8,128)(2,1)} %bitcast.11, ...), custom_call_target="tpu_custom_call" | custom-call | tf_op jit(solution)/shard_map/experts/pallas_call | solution.py:757
  196.3 2.0 settle.1
